TPU v7x, 32 devices: a whole 2x2x4 slice. The times are simulated.
32 devices in a mesh: sp: 8 (over z, y), tp: 4 (over x, core).
Axes of the slice: x: 2, y: 2, z: 4, core: 2. Of those that a mesh axis runs over, the one named last changes fastest.
Arguments:
- stream_in: bfloat16 [4096, 2048], P(('sp', 'tp')), may hold values from -6 to 6
- stream_cot: bfloat16 [4096, 2048], P(('sp', 'tp')), may hold values from -4 to 4
- route_ids: int32 [4096, 2], P('sp'), may hold values from 0 to 7, all different within a row; in each aligned block of 128 rows (0 to 127, 128 to 255, ...) at most 40 rows name the same one
- route_wts: float32 [4096, 2], P('sp'), may hold values from 0.2 to 0.8
- norm_gain: float32 [2048], replicated, may hold values from 0.1 to 1.9
- w_gate: bfloat16 [8, 2048, 1024], P('sp', None, 'tp'), may hold values from -0.125 to 0.125
- w_up: bfloat16 [8, 2048, 1024], P('sp', None, 'tp'), may hold values from -0.125 to 0.125
- w_down: bfloat16 [8, 1024, 2048], P('sp', 'tp'), may hold values from -0.1875 to 0.1875
- out_proj: bfloat16 [1024, 2048], P('tp'), may hold values from -0.1875 to 0.1875
- conv_b: bfloat16 [4096, 1024], P('sp', 'tp'), may hold values from -6 to 6
- conv_c: bfloat16 [4096, 1024], P('sp', 'tp'), may hold values from -6 to 6
- conv_h: bfloat16 [4096, 1024], P('sp', 'tp'), may hold values from -6 to 6
- conv_taps: float32 [3, 1024], P(None, 'tp'), may hold values from -3.5 to 3.5
Outputs:
- grad_gate: float32 [8, 2048, 1024], P('sp', None, 'tp')
- grad_up: float32 [8, 2048, 1024], P('sp', None, 'tp')
- grad_down: float32 [8, 1024, 2048], P('sp', 'tp')
- proj_grad: float32 [2048, 1024], P('sp', 'tp')
- grad_b: bfloat16 [4096, 1024], P('sp', 'tp')
- grad_c: bfloat16 [4096, 1024], P('sp', 'tp')
- grad_h: bfloat16 [4096, 1024], P('sp', 'tp')
Inputs may be any that keep to these rules, and one draw needn't show every extreme that they name: `route_ids`: the 2 experts of a token differ. In each aligned block of 128 tokens no expert is named by more than 40 pairs, and in every draw some expert is named by exactly 40 pairs of some block.
All inputs are finite; a program needn't handle non-finite values.
Results may differ from a plain program's by a relative error of at most 0.015.
Values may be sent and summed in bfloat16 or wider, within the bound.
A program may use at most 128 MiB of HBM per device.

v0:
```python
import jax
import jax.numpy as jnp
from jax import lax
from jax.sharding import PartitionSpec as P

epsilon = 1e-06


def from_behind(value, axis, steps):
    count = lax.axis_size(axis)
    initial, last = (max(0, -steps), min(count, count - steps))
    return lax.ppermute(value, axis, [(source, source + steps) for source in range(initial, last)])


def slot_ranks(pair_ids, experts):
    onehot = (pair_ids[..., None] == jnp.arange(experts, dtype=jnp.int32)).astype(jnp.int32)
    ranks = jnp.cumsum(onehot, axis=-2) - 1
    return jnp.sum(ranks * onehot, axis=-1)


def expert_work(rows_in, cot_rows, gate_w, up_w, down_w):
    gate_pre = jnp.dot(rows_in, gate_w, preferred_element_type=jnp.float32)
    up_pre = jnp.dot(rows_in, up_w, preferred_element_type=jnp.float32)
    gate_sig = jax.nn.sigmoid(gate_pre)
    gate_act = gate_pre * gate_sig
    hidden = (gate_act * up_pre).astype(jnp.bfloat16)
    down_grad = lax.dot_general(
        hidden, cot_rows, (((0,), (0,)), ((), ())), preferred_element_type=jnp.float32
    )
    grad_hidden = lax.dot_general(
        cot_rows, down_w, (((1,), (1,)), ((), ())), preferred_element_type=jnp.float32
    )
    up_grad = (grad_hidden * gate_act).astype(jnp.bfloat16)
    gate_grad = (grad_hidden * up_pre * gate_sig * (1.0 + gate_pre * (1.0 - gate_sig))).astype(
        jnp.bfloat16
    )
    gate_wgrad = lax.dot_general(
        rows_in, gate_grad, (((0,), (0,)), ((), ())), preferred_element_type=jnp.float32
    )
    up_wgrad = lax.dot_general(
        rows_in, up_grad, (((0,), (0,)), ((), ())), preferred_element_type=jnp.float32
    )
    grads_pair = jnp.stack([gate_grad, up_grad], axis=1)
    weights_pair = jnp.stack([gate_w, up_w], axis=1)
    back_rows = lax.dot_general(
        grads_pair, weights_pair, (((1, 2), (1, 2)), ((), ())), preferred_element_type=jnp.float32
    ).astype(jnp.bfloat16)
    return (gate_wgrad, up_wgrad, down_grad, back_rows)


def shards(
    stream_in,
    stream_cot,
    route_ids,
    route_wts,
    norm_gain,
    w_gate,
    w_up,
    w_down,
    out_proj,
    conv_b,
    conv_c,
    conv_h,
    conv_taps,
):
    tp_count = lax.axis_size("tp")
    sp_count = lax.axis_size("sp")
    tp_index = lax.axis_index("tp")
    tok_rows, model_width = stream_in.shape
    top_count = route_ids.shape[1]
    capacity = max(2, 5 * top_count * tok_rows // (4 * sp_count))
    inputs = stream_in.astype(jnp.float32)
    inv_rms = lax.rsqrt(jnp.mean(inputs * inputs, axis=1, keepdims=True) + epsilon)
    scaled = inputs * inv_rms
    normed = (scaled * norm_gain[None, :]).astype(jnp.bfloat16)
    group_ids = route_ids.reshape(tp_count, top_count * tok_rows)
    group_slots = slot_ranks(group_ids, sp_count)
    own_ids = lax.dynamic_index_in_dim(group_ids, tp_index, 0, keepdims=False)
    own_slots = lax.dynamic_index_in_dim(group_slots, tp_index, 0, keepdims=False)
    own_places = own_ids * capacity + own_slots
    own_wts = lax.dynamic_slice_in_dim(route_wts, tp_index * tok_rows, tok_rows, 0)
    own_weighted = (own_wts[:, :, None] * stream_cot.astype(jnp.float32)[:, None, :]).astype(
        jnp.bfloat16
    )
    own_weighted = own_weighted.reshape(-1, model_width)
    own_rows = jnp.repeat(normed, top_count, axis=0)
    buffer_rows = (
        jnp.zeros((sp_count * capacity, model_width), jnp.bfloat16).at[own_places].set(own_rows)
    )
    buffer_cot = (
        jnp.zeros((sp_count * capacity, model_width), jnp.bfloat16).at[own_places].set(own_weighted)
    )
    buffer_rows = buffer_rows.reshape(sp_count, capacity, model_width)
    buffer_cot = buffer_cot.reshape(sp_count, capacity, model_width)
    landed_rows, landed_cot = (
        lax.all_to_all(buffer_rows, "sp", split_axis=0, concat_axis=0, tiled=True),
        lax.all_to_all(buffer_cot, "sp", split_axis=0, concat_axis=0, tiled=True),
    )
    arrived_rows, arrived_cot = (
        lax.all_gather(landed_rows, "tp", axis=1, tiled=True),
        lax.all_gather(landed_cot, "tp", axis=1, tiled=True),
    )
    gate_wgrad, up_wgrad, down_grad, back_rows = expert_work(
        arrived_rows.reshape(-1, model_width),
        arrived_cot.reshape(-1, model_width),
        w_gate[0],
        w_up[0],
        w_down[0],
    )
    back_rows = back_rows.reshape(sp_count, tp_count * capacity, model_width)
    summed_back = lax.psum_scatter(
        back_rows.astype(jnp.float32).astype(jnp.bfloat16), "tp", scatter_dimension=1, tiled=True
    )
    returned = lax.all_to_all(summed_back, "sp", split_axis=0, concat_axis=0, tiled=True)
    picked = returned.reshape(sp_count * capacity, model_width)[own_places]
    grad_normed = jnp.sum(
        picked.astype(jnp.float32).reshape(tok_rows, top_count, model_width), axis=1
    )
    q_term = grad_normed * norm_gain[None, :]
    stream_grad = (
        stream_cot.astype(jnp.float32)
        + inv_rms * (q_term - scaled * jnp.mean(q_term * scaled, axis=1, keepdims=True))
    ).astype(jnp.bfloat16)
    group_grad = lax.all_gather(stream_grad, "tp", axis=0, tiled=True)
    grad_mix = lax.dot_general(
        group_grad, out_proj, (((1,), (1,)), ((), ())), preferred_element_type=jnp.float32
    ).astype(jnp.bfloat16)
    rim_prev = from_behind(jnp.stack([conv_c[-2:], conv_h[-2:]]), "sp", 1)
    gate_ext = jnp.concatenate([rim_prev[0], conv_c], axis=0).astype(jnp.float32)
    value_ext = jnp.concatenate([rim_prev[1], conv_h], axis=0).astype(jnp.float32)
    conv_in = gate_ext * value_ext
    conv_out = (
        conv_taps[0][None, :] * conv_in[:-2]
        + conv_taps[1][None, :] * conv_in[1:-1]
        + conv_taps[2][None, :] * conv_in[2:]
    )
    mixed = (conv_b.astype(jnp.float32) * conv_out).astype(jnp.bfloat16)
    proj_grad = lax.psum_scatter(
        lax.dot_general(
            group_grad, mixed, (((0,), (0,)), ((), ())), preferred_element_type=jnp.float32
        ),
        "sp",
        scatter_dimension=0,
        tiled=True,
    )
    grad_b = (grad_mix.astype(jnp.float32) * conv_out).astype(jnp.bfloat16)
    rim_next = from_behind(jnp.stack([grad_mix[:2], conv_b[:2]]), "sp", -1)
    conv_grad = grad_mix.astype(jnp.float32) * conv_b.astype(jnp.float32)
    next_grad = rim_next[0].astype(jnp.float32) * rim_next[1].astype(jnp.float32)
    grad_ext = jnp.concatenate([conv_grad, next_grad], axis=0)
    grad_in = (
        conv_taps[2][None, :] * grad_ext[:-2]
        + conv_taps[1][None, :] * grad_ext[1:-1]
        + conv_taps[0][None, :] * grad_ext[2:]
    )
    grad_c = (grad_in * conv_h.astype(jnp.float32)).astype(jnp.bfloat16)
    grad_h = (grad_in * conv_c.astype(jnp.float32)).astype(jnp.bfloat16)
    return (gate_wgrad[None], up_wgrad[None], down_grad[None], proj_grad, grad_b, grad_c, grad_h)


def solution(mesh):
    in_specs = (
        P(("sp", "tp"), None),
        P(("sp", "tp"), None),
        P("sp", None),
        P("sp", None),
        P(),
        P("sp", None, "tp"),
        P("sp", None, "tp"),
        P("sp", "tp", None),
        P("tp", None),
        P("sp", "tp"),
        P("sp", "tp"),
        P("sp", "tp"),
        P(None, "tp"),
    )
    out_specs = (
        P("sp", None, "tp"),
        P("sp", None, "tp"),
        P("sp", "tp", None),
        P("sp", "tp"),
        P("sp", "tp"),
        P("sp", "tp"),
        P("sp", "tp"),
    )
    return jax.shard_map(shards, mesh=mesh, in_specs=in_specs, out_specs=out_specs, check_vma=False)
```

profile of v0, /device:TPU:0, one launch (start us, length us, event | category | flops | bytes accessed | tf_op | source)
XLA Modules:
  0.0 350.9 jit_solution(16371966378131730908)
XLA Ops:
  7.3 0.9 copy.27
  8.2 0.2 reshape.110
  8.4 0.2 eq.26
  8.5 1.2 fusion.16
  9.8 2.3 reduce-window.6
  12.3 0.2 fusion.10
  12.5 0.6 broadcast_in_dim.8
  13.1 0.4 reshape.132
  13.7 2.5 scatter_custom_fusion
  16.2 38.6 %all_to_all.15 = bf16[8,40,2048]{2,1,0:T(8,128)(2,1)} all-to-all(bf16[8,40,2048]{2,1,0:T(8,128)(2,1)S(1)} %bitcast.84), channel_id=1, replica_groups=mesh['sp'=8,'tp'=4] {'sp'}, dimensions={0} | all-to-all | bytes 2621440 | tf_op jit(solution)/shard_map/all_to_all | solution.py:96
  54.9 0.7 constant_dynamic-slice_fusion
  55.8 2.1 mul.184
  57.9 2.4 mul.185
  60.4 3.9 %scatter_custom_fusion.1 = bf16[320,2048]{1,0:T(8,128)(2,1)S(1)} fusion(s32[256]{0:T(256)S(1)} %bitcast.88, f32[256,2048]{1,0:T(8,128)} %mul.185, f32[256]{0:T(256)S(1)} %mul.182, bf16[]{:T(256)} %constant.13.clone.1), kind=kCustom, calls=%fused_computation.32 | custom fusion | flops 1048576 | bytes 3408898 | tf_op jit(solution)/shard_map/scatter | solution.py:91
  64.3 34.3 %all_to_all.16 = bf16[8,40,2048]{2,1,0:T(8,128)(2,1)} all-to-all(bf16[8,40,2048]{2,1,0:T(8,128)(2,1)S(1)} %bitcast.83), channel_id=1, replica_groups=mesh['sp'=8,'tp'=4] {'sp'}, dimensions={0} | all-to-all | bytes 2621440 | tf_op jit(solution)/shard_map/all_to_all | solution.py:97
  98.6 0.2 reduce-scatter.7.cloned.1.call-start
  98.8 0.9 copy-done.12
  99.8 5.2 %fusion.18 = f32[1280,256]{1,0:T(8,128)} fusion(bf16[1280,2048]{1,0:T(8,128)(2,1)} %bitcast.96, bf16[1,2048,256]{2,1,0:T(8,128)(2,1)S(1)} %copy-done.12), kind=kOutput, calls=%fused_computation.33 | convolution fusion | flops 1342177280 | bytes 7602176 | tf_op jit(solution)/shard_map/dot_general | solution.py:22
  105.0 2.6 fusion.20
  107.6 30.5 %all-gather.6.cloned.1.call-done = bf16[8,160,2048]{2,1,0:T(8,128)(2,1)} async-done(((bf16[8,40,2048]{2,1,0:T(8,128)(2,1)}), bf16[8,160,2048]{2,1,0:T(8,128)(2,1)}) %all-gather.6.cloned.1.call-update) | async-done | bytes 5242896 | tf_op jit(solution)/shard_map/all_gather | solution.py:101
  138.1 5.1 %multiply_convert_fusion.2 = (bf16[1280,256]{1,0:T(8,128)(2,1)S(1)}, bf16[1280,256]{1,0:T(8,128)(2,1)S(1)}) fusion(f32[1280,256]{1,0:T(8,128)} %fusion.18, f32[1280,256]{1,0:T(8,128)} %fusion.20, bf16[1280,2048]{1,0:T(8,128)(2,1)} %bitcast.102, bf16[1,256,2048]{2,1,0:T(8,128)(2,1)S(1)} %copy-done), kind=kOutput, calls=%fused_computation.20 | convolution fusion | flops 1346437120 | bytes 10223616 | tf_op jit(solution)/shard_map/dot_general | solution.py:30
  143.3 3.2 bitcast_convert_fusion
  146.5 2.8 copy.34
  149.3 51.5 %reduce-scatter.7.cloned.1.call-done = bf16[40,16384]{1,0:T(8,128)(2,1)} async-done(((bf16[160,16384]{1,0:T(8,128)(2,1)}), bf16[40,16384]{1,0:T(8,128)(2,1)}) %reduce-scatter.7.cloned.1.call-update) | async-done | bytes 1310736
  200.8 2.0 copy.35
  202.8 1.8 copy.33
  204.6 5.5 %all-to-all-start.2 = ((bf16[8,40,2048]{2,1,0:T(8,128)(2,1)}), bf16[8,40,2048]{2,1,0:T(8,128)(2,1)S(1)}, u32[]{:S(2)}, u32[]{:S(2)}) async-start(bf16[8,40,2048]{2,1,0:T(8,128)(2,1)} %copy.33), calls=%async_computation.2 | async-start | bytes 2621440 | tf_op jit(solution)/shard_map/all_to_all | solution.py:114
  210.1 0.3 all-gather.8.cloned.1.call-start
  210.4 31.0 %all-to-all-done.2 = bf16[8,40,2048]{2,1,0:T(8,128)(2,1)S(1)} async-done(((bf16[8,40,2048]{2,1,0:T(8,128)(2,1)}), bf16[8,40,2048]{2,1,0:T(8,128)(2,1)S(1)}, u32[]{:S(2)}, u32[]{:S(2)}) %all-to-all-start.2) | async-done | bytes 1310752 | tf_op jit(solution)/shard_map/all_to_all | solution.py:114
  241.3 1.4 gather_fusion
  242.7 1.3 reshape.119
  244.1 2.8 reduce_sum.38
  246.9 1.4 fusion.11
  248.3 1.2 fusion.15
  249.7 3.5 collective-permute-start
  253.2 1.3 collective-permute-done
  254.6 15.8 %all-gather.8.cloned.1.call-done = bf16[512,2048]{1,0:T(8,128)(2,1)} async-done(((bf16[128,2048]{1,0:T(8,128)(2,1)}), bf16[512,2048]{1,0:T(8,128)(2,1)}) %all-gather.8.cloned.1.call-update) | async-done | bytes 2097168 | tf_op jit(solution)/shard_map/all_gather | solution.py:124
  270.4 3.3 fusion.33
  273.7 2.1 fusion.37
  275.9 1.0 copy-done.18
  277.0 5.5 %convolution_bitcast_fusion.1 = f32[1,2048,256]{2,1,0:T(8,128)} fusion(bf16[1280,2048]{1,0:T(8,128)(2,1)} %bitcast.97, bf16[1280,256]{1,0:T(8,128)(2,1)S(1)} %copy-done.18), kind=kOutput, calls=%fused_computation.5 | convolution fusion | flops 1342177280 | bytes 7995392 | tf_op jit(solution)/shard_map/dot_general | solution.py:40
  282.5 5.6 %convolution_bitcast_fusion = f32[1,256,2048]{2,1,0:T(8,128)} fusion(bf16[1280,2048]{1,0:T(8,128)(2,1)} %bitcast.103, f32[1280,256]{1,0:T(8,128)S(1)} %copy-done.20, f32[1280,256]{1,0:T(8,128)S(1)} %copy-done.19), kind=kOutput, calls=%fused_computation.4 | convolution fusion | flops 1344143360 | bytes 9961472 | tf_op jit(solution)/shard_map/dot_general | solution.py:27
  288.2 1.3 collective-permute-start.1
  289.5 3.0 convolution_bitcast_fusion.2
  292.5 1.1 collective-permute-done.1
  293.7 0.9 multiply_convert_fusion.6
  294.6 0.8 multiply_convert_fusion.7
  295.3 49.1 %reduce-scatter.5.cloned.1.call-done = f32[256,256]{1,0:T(8,128)} async-done(((f32[2048,256]{1,0:T(8,128)}), f32[256,256]{1,0:T(8,128)}) %reduce-scatter.5.cloned.1.call-update) | async-done | bytes 262160 | tf_op jit(solution)/shard_map/reduce_scatter | solution.py:138
  (76 shorter events, 1.1 us)
Async XLA Ops:
  7.2 130.9 %copy-start = (bf16[1,256,2048]{2,1,0:T(8,128)(2,1)S(1)}, bf16[1,256,2048]{2,1,0:T(8,128)(2,1)}, u32[]{:S(2)}) copy-start(bf16[1,256,2048]{2,1,0:T(8,128)(2,1)} %param.20) | copy-start | bytes 3145732
  7.2 5.1 %copy-start.2 = (bf16[128,2048]{1,0:T(8,128)(2,1)S(1)}, bf16[128,2048]{1,0:T(8,128)(2,1)}, u32[]{:S(2)}) copy-start(bf16[128,2048]{1,0:T(8,128)(2,1)} %param.13) | copy-start | bytes 1572868
  7.2 5.1 %copy-start.9 = (f32[2048]{0:T(1024)S(1)}, f32[2048]{0:T(1024)}, u32[]{:S(2)}) copy-start(f32[2048]{0:T(1024)} %param.17) | copy-start | bytes 24580
  7.2 91.6 %all-gather.4.cloned.1.call-start = ((), (), s32[]{:S(2)}) async-start(), calls=%async_computation.5 | async-start | bytes 6553600 | tf_op jit(solution)/shard_map/all_gather | solution.py:100
  54.8 83.3 %all-gather.6.cloned.1.call-start = ((), (), s32[]{:S(2)}) async-start(), calls=%async_computation.6 | async-start | bytes 6553600 | tf_op jit(solution)/shard_map/all_gather | solution.py:101
  98.6 1.2 copy-start.12
  98.6 102.2 %reduce-scatter.7.cloned.1.call-start = ((), (), s32[]{:S(2)}) async-start(), calls=%async_computation.9 | async-start | bytes 6553600
  99.8 5.2 %copy-start.11 = (bf16[8,160,2048]{2,1,0:T(8,128)(2,1)S(1)}, bf16[8,160,2048]{2,1,0:T(8,128)(2,1)}, u32[]{:S(2)}) copy-start(bf16[8,160,2048]{2,1,0:T(8,128)(2,1)} %all-gather.4.cloned.1.call-done) | copy-start | bytes 15728644
  99.8 5.2 %copy-start.13 = (bf16[1,2048,256]{2,1,0:T(8,128)(2,1)S(1)}, bf16[1,2048,256]{2,1,0:T(8,128)(2,1)}, u32[]{:S(2)}) copy-start(bf16[1,2048,256]{2,1,0:T(8,128)(2,1)} %param.19) | copy-start | bytes 3145732
  143.3 3.2 copy-start.15
  143.3 3.2 copy-start.17
  204.6 36.7 %all-to-all-start.2 = ((bf16[8,40,2048]{2,1,0:T(8,128)(2,1)}), bf16[8,40,2048]{2,1,0:T(8,128)(2,1)S(1)}, u32[]{:S(2)}, u32[]{:S(2)}) async-start(bf16[8,40,2048]{2,1,0:T(8,128)(2,1)} %copy.33), calls=%async_computation.2 | async-start | bytes 2621440 | tf_op jit(solution)/shard_map/all_to_all | solution.py:114
  210.1 60.3 %all-gather.8.cloned.1.call-start = ((), (), s32[]{:S(2)}) async-start(), calls=%async_computation.7 | async-start | bytes 2621440 | tf_op jit(solution)/shard_map/all_gather | solution.py:124
  246.8 1.5 copy-start.3
  246.8 1.5 copy-start.5
  248.3 1.3 copy-start.6
  248.3 1.3 copy-start.7
  248.3 4.8 %copy-start.10 = (f32[3,256]{1,0:T(4,128)S(1)}, f32[3,256]{1,0:T(4,128)}, u32[]{:S(2)}) copy-start(f32[3,256]{1,0:T(4,128)} %param.25) | copy-start | bytes 9220
  249.5 20.9 %copy-start.8 = (bf16[512,256]{1,0:T(8,128)(2,1)S(1)}, bf16[512,256]{1,0:T(8,128)(2,1)}, u32[]{:S(2)}) copy-start(bf16[512,256]{1,0:T(8,128)(2,1)} %param.22) | copy-start | bytes 786436
  249.5 20.9 %copy-start.14 = (bf16[256,2048]{1,0:T(8,128)(2,1)S(1)}, bf16[256,2048]{1,0:T(8,128)(2,1)}, u32[]{:S(2)}) copy-start(bf16[256,2048]{1,0:T(8,128)(2,1)} %param.21) | copy-start | bytes 3145732
  249.6 94.8 %reduce-scatter.5.cloned.1.call-start = ((), (), s32[]{:S(2)}) async-start(), calls=%async_computation.8 | async-start | bytes 2359296 | tf_op jit(solution)/shard_map/reduce_scatter | solution.py:138
  249.7 4.8 %collective-permute-start = (bf16[2,2,256]{2,1,0:T(2,128)(2,1)S(1)}, bf16[2,2,256]{2,1,0:T(2,128)(2,1)S(1)}, u32[]{:S(2)}, u32[]{:S(2)}) collective-permute-start(bf16[2,2,256]{2,1,0:T(2,128)(2,1)S(1)} %pad_maximum_fusion.1), channel_id=1, source_target_pairs={{0,4},{4,8},{8,12},{12,16},{16,20},{20,24},{24,28},{1,5},{5,9},{9,... | collective-permute-start | bytes 6152 | tf_op jit(solution)/shard_map/ppermute | solution.py:12
  270.4 3.3 copy-start.4
  275.9 1.1 copy-start.18
  276.9 5.6 %copy-start.19 = (f32[1280,256]{1,0:T(8,128)S(1)}, f32[1280,256]{1,0:T(8,128)}, u32[]{:S(2)}) copy-start(f32[1280,256]{1,0:T(8,128)} %fusion.18) | copy-start | bytes 3932164
  276.9 5.6 %copy-start.20 = (f32[1280,256]{1,0:T(8,128)S(1)}, f32[1280,256]{1,0:T(8,128)}, u32[]{:S(2)}) copy-start(f32[1280,256]{1,0:T(8,128)} %fusion.20) | copy-start | bytes 3932164
  276.9 12.5 %slice-start = ((s8[5242880]{0:T(1024)(128)(4,1)}), s8[4194304]{0:T(1024)(128)(4,1)S(1)}, s32[]{:S(2)}) async-start(s8[5242880]{0:T(1024)(128)(4,1)} %bitcast.99), calls=%async_computation.10 | async-start | bytes 8388608
  282.5 7.0 %slice-start.1 = ((s8[5242880]{0:T(1024)(128)(4,1)}), s8[1048576]{0:T(1024)(128)(4,1)S(1)}, s32[]{:S(2)}) async-start(s8[5242880]{0:T(1024)(128)(4,1)} %bitcast.99), calls=%async_computation.11 | async-start | bytes 2097152
  282.5 7.0 %copy-start.16 = (bf16[1280,256]{1,0:T(8,128)(2,1)S(1)}, bf16[1280,256]{1,0:T(8,128)(2,1)}, u32[]{:S(2)}) copy-start(bf16[1280,256]{1,0:T(8,128)(2,1)} %copy-done.15) | copy-start | bytes 1966084
  288.2 5.5 %collective-permute-start.1 = (bf16[2,2,256]{2,1,0:T(2,128)(2,1)S(1)}, bf16[2,2,256]{2,1,0:T(2,128)(2,1)S(1)}, u32[]{:S(2)}, u32[]{:S(2)}) collective-permute-start(bf16[2,2,256]{2,1,0:T(2,128)(2,1)S(1)} %pad_maximum_fusion.2), channel_id=1, source_target_pairs={{4,0},{8,4},{12,8},{16,12},{20,16},{24,20},{28,24},{5,1},{9,5},{13... | collective-permute-start | bytes 6152 | tf_op jit(solution)/shard_map/ppermute | solution.py:12
  293.7 50.7 %copy-start.1 = (bf16[1,256,2048]{2,1,0:T(8,128)(2,1)S(1)}, bf16[1,256,2048]{2,1,0:T(8,128)(2,1)}, u32[]{:S(2)}) copy-start(bf16[1,256,2048]{2,1,0:T(8,128)(2,1)} %param.20) | copy-start | bytes 3145732
Sparse Core Ops, SparseCore 0:
  54.9 39.4 all-gather.3
  98.7 39.3 all-gather.5
  149.4 51.3 reduce-scatter.6
  249.7 20.6 all-gather.7
  276.0 68.3 reduce-scatter.4
where the time goes:
time: 351 us
  waiting for transfers between devices  180 us (51%)
  blocking collectives  72.9 us (21%)
  matrix products  35.8 us (10%)
  local copies, waits for them, and re-layouts  21.9 us (6%)
  other arithmetic  14.9 us (4%)
  between operations  14.2 us (4%)
  starting transfers between devices  10.9 us (3%)
    unnamed x6, waiting for transfers between devices  51.6 us
    reduce_scatter x1, waiting for transfers between devices, shards(): lax.psum_scatter(lax.dot_general(group_grad, mixed, (((0,), (0,)), ((), (...  49.1 us
    all_to_all x1, blocking collectives, shards(): lax.all_to_all(buffer_rows, 'sp', split_axis=0, concat_axis=0, tiled=True)  38.6 us
    all_to_all x1, blocking collectives, shards(): lax.all_to_all(buffer_cot, 'sp', split_axis=0, concat_axis=0, tiled=True)  34.3 us
    all_to_all x1, waiting for transfers between devices, shards(): lax.all_to_all(summed_back, 'sp', split_axis=0, concat_axis=0, tiled=True)  31 us
    all_gather x1, waiting for transfers between devices, shards(): lax.all_gather(landed_cot, 'tp', axis=1, tiled=True)  30.5 us
    all_gather x1, waiting for transfers between devices, shards(): group_grad = lax.all_gather(stream_grad, 'tp', axis=0, tiled=True)  15.8 us
    unnamed x50, local copies, waits for them, and re-layouts  9.63 us
  transfers between devices with their start and end apart: 8, of which 7 were waited for; matrix products, arithmetic and copies ran while one was open for 9% of the time, Pallas kernels for 0%

commit v1 on v0

--- a/solution.py
+++ b/solution.py
@@ -1,9 +1,369 @@
+import functools
+
 import jax
 import jax.numpy as jnp
 from jax import lax
+from jax.experimental import pallas as pl
+from jax.experimental.pallas import tpu as pltpu
 from jax.sharding import PartitionSpec as P
 
 epsilon = 1e-06
+
+
+def here():
+    return lax.axis_index("sp"), lax.axis_index("tp")
+
+
+def greet(sp_count, tp_count):
+    sp_at, tp_at = here()
+    half = tp_count // 2
+    barrier = pltpu.get_barrier_semaphore()
+
+    def hail(sp_to, tp_to):
+        pl.semaphore_signal(
+            barrier, inc=1, device_id=(sp_to, tp_to), device_id_type=pl.DeviceIdType.MESH
+        )
+
+    def hail_row(step, carry):
+        hail(lax.rem(sp_at + step, sp_count), tp_at)
+        return carry
+
+    lax.fori_loop(1, sp_count, hail_row, 0)
+    for step in range(1, half):
+        hail(sp_at, pair_peer(tp_at, step, half))
+    hail(sp_at, mate_of(tp_at))
+    pl.semaphore_wait(barrier, sp_count - 1 + half)
+
+
+def pair_peer(tp_at, step, half):
+    return lax.rem(tp_at // 2 + step, half) * 2 + lax.rem(tp_at, 2)
+
+
+def mate_of(tp_at):
+    return tp_at + 1 - 2 * lax.rem(tp_at, 2)
+
+
+def remote(source, target, send_sem, recv_sem, sp_to, tp_to):
+    return pltpu.make_async_remote_copy(
+        src_ref=source,
+        dst_ref=target,
+        send_sem=send_sem,
+        recv_sem=recv_sem,
+        device_id=(sp_to, tp_to),
+        device_id_type=pl.DeviceIdType.MESH,
+    )
+
+
+def loop(first, last, body):
+    def step(index, carry):
+        body(index)
+        return carry
+
+    lax.fori_loop(first, last, step, 0)
+
+
+def spread_kernel(sp_count, tp_count, exchanged, gathered, *refs):
+    count = exchanged + gathered
+    sources, results = refs[:count], refs[count : 2 * count]
+    own_sem, row_send, row_recv, pair_send, pair_recv, mate_send, mate_recv, last_send, last_recv = (
+        refs[2 * count :]
+    )
+    sp_at, tp_at = here()
+    half = tp_count // 2
+    mate = mate_of(tp_at)
+
+    def origin(step):
+        return lax.rem(sp_at + sp_count - step, sp_count)
+
+    def slot_of(which, step, tp_from):
+        if which < exchanged:
+            return results[which].at[origin(step), tp_from]
+        return results[which].at[tp_from]
+
+    def own_block(which):
+        return sources[which].at[sp_at] if which < exchanged else sources[which]
+
+    def row_copy(which, step):
+        to = lax.rem(sp_at + step, sp_count)
+        return remote(
+            sources[which].at[to],
+            results[which].at[sp_at, tp_at],
+            row_send.at[which, step],
+            row_recv.at[which, step],
+            to,
+            tp_at,
+        )
+
+    def row_arrival(which, step):
+        return remote(
+            own_block(which),
+            slot_of(which, step, tp_at),
+            row_send.at[which, step],
+            row_recv.at[which, step],
+            origin(step),
+            tp_at,
+        )
+
+    def pair_copy(which, step, hop, source, tp_from):
+        return remote(
+            source,
+            slot_of(which, step, tp_from),
+            pair_send.at[which, step, hop],
+            pair_recv.at[which, step, hop],
+            sp_at,
+            pair_peer(tp_at, hop, half),
+        )
+
+    def mate_copy(which, step, source, tp_from):
+        return remote(
+            source,
+            slot_of(which, step, tp_from),
+            mate_send.at[which, step],
+            mate_recv.at[which, step],
+            sp_at,
+            mate,
+        )
+
+    def last_copy(which, step, hop, tp_from):
+        return remote(
+            slot_of(which, step, tp_from),
+            slot_of(which, step, tp_from),
+            last_send.at[which, step, hop],
+            last_recv.at[which, step, hop],
+            sp_at,
+            mate,
+        )
+
+    def pair_source(hop):
+        return pair_peer(tp_at, half - hop, half)
+
+    def pass_on(which, step, source):
+        for hop in range(1, half):
+            pair_copy(which, step, hop, source, tp_at).start()
+        mate_copy(which, step, source, tp_at).start()
+
+    def pass_last(which, step):
+        for hop in range(1, half):
+            origin_tp = pair_source(hop)
+            pair_copy(which, step, hop, own_block(which), origin_tp).wait_recv()
+            last_copy(which, step, hop, origin_tp).start()
+
+    greet(sp_count, tp_count)
+    for which in range(exchanged):
+        loop(1, sp_count, lambda step: row_copy(which, step).start())
+    locals_ = [
+        pltpu.make_async_copy(own_block(which), slot_of(which, 0, tp_at), own_sem.at[which])
+        for which in range(count)
+    ]
+    for copy in locals_:
+        copy.start()
+    for which in reversed(range(count)):
+        pass_on(which, 0, own_block(which))
+
+    for which in range(exchanged, count):
+        pass_last(which, 0)
+    for which in range(exchanged):
+
+        def relay(step):
+            row_arrival(which, step).wait_recv()
+            pass_on(which, step, slot_of(which, step, tp_at))
+            pass_last(which, step - 1)
+
+        loop(1, sp_count, relay)
+        pass_last(which, sp_count - 1)
+
+    for copy in locals_:
+        copy.wait()
+    for which in range(count):
+        steps = sp_count if which < exchanged else 1
+
+        def finish(step):
+            for hop in range(1, half):
+                pair_copy(which, step, hop, own_block(which), tp_at).wait_send()
+                last_copy(which, step, hop, pair_source(hop)).wait_send()
+                last_copy(
+                    which, step, hop, mate_of(pair_source(hop))
+                ).wait_recv()
+            mate_copy(which, step, own_block(which), tp_at).wait_send()
+            mate_copy(which, step, own_block(which), mate).wait_recv()
+
+        loop(0, steps, finish)
+        if which < exchanged:
+            loop(1, sp_count, lambda step: row_copy(which, step).wait_send())
+
+
+def spread(sp_count, tp_count, exchanged, gathered, collective_id):
+    arrays = list(exchanged) + list(gathered)
+    count = len(arrays)
+    half = tp_count // 2
+    shapes = [
+        jax.ShapeDtypeStruct((sp_count, tp_count) + value.shape[1:], value.dtype)
+        for value in exchanged
+    ] + [jax.ShapeDtypeStruct((tp_count,) + value.shape, value.dtype) for value in gathered]
+    sems = pltpu.SemaphoreType.DMA
+    return pl.pallas_call(
+        functools.partial(spread_kernel, sp_count, tp_count, len(exchanged), len(gathered)),
+        out_shape=tuple(shapes),
+        in_specs=[pl.BlockSpec(memory_space=pltpu.VMEM)] * count,
+        out_specs=tuple([pl.BlockSpec(memory_space=pl.ANY)] * count),
+        scratch_shapes=[sems((count,))]
+        + [sems((count, sp_count))] * 2
+        + [sems((count, sp_count, half))] * 2
+        + [sems((count, sp_count))] * 2
+        + [sems((count, sp_count, half))] * 2,
+        compiler_params=pltpu.CompilerParams(collective_id=collective_id, has_side_effects=True),
+    )(*arrays)
+
+
+def bring_kernel(
+    sp_count,
+    tp_count,
+    partial_ref,
+    result_ref,
+    own,
+    from_mate,
+    from_pair,
+    final,
+    load_sem,
+    mate_send,
+    mate_recv,
+    pair_send,
+    pair_recv,
+    row_send,
+    row_recv,
+    own_sem,
+):
+    sp_at, tp_at = here()
+    half = tp_count // 2
+    pair_at, side = tp_at // 2, lax.rem(tp_at, 2)
+    mate = mate_of(tp_at)
+
+    def target(step):
+        return lax.rem(sp_at + step, sp_count)
+
+    def load(step):
+        return pltpu.make_async_copy(
+            partial_ref.at[target(step), :, side], own.at[step], load_sem.at[step]
+        )
+
+    def mate_copy(step):
+        return remote(
+            partial_ref.at[target(step), :, 1 - side],
+            from_mate.at[step],
+            mate_send.at[step],
+            mate_recv.at[step],
+            sp_at,
+            mate,
+        )
+
+    def pair_copy(step, hop):
+        return remote(
+            own.at[step, lax.rem(pair_at + hop, half)],
+            from_pair.at[step, hop - 1],
+            pair_send.at[step, hop],
+            pair_recv.at[step, hop],
+            sp_at,
+            pair_peer(tp_at, hop, half),
+        )
+
+    def row_copy(step):
+        return remote(
+            final.at[step],
+            result_ref.at[sp_at],
+            row_send.at[step],
+            row_recv.at[step],
+            target(step),
+            tp_at,
+        )
+
+    def row_arrival(step):
+        came = lax.rem(sp_at + sp_count - step, sp_count)
+        return remote(
+            final.at[step],
+            result_ref.at[came],
+            row_send.at[step],
+            row_recv.at[step],
+            came,
+            tp_at,
+        )
+
+    greet(sp_count, tp_count)
+
+    def begin(step):
+        mate_copy(step).start()
+        load(step).start()
+
+    loop(1, sp_count, begin)
+    begin(0)
+
+    def add_mate(step):
+        load(step).wait()
+        mate_copy(step).wait_recv()
+        own[step] = (
+            own[step].astype(jnp.float32) + from_mate[step].astype(jnp.float32)
+        ).astype(jnp.bfloat16)
+        for hop in range(1, half):
+            pair_copy(step, hop).start()
+
+    loop(1, sp_count, add_mate)
+    add_mate(0)
+
+    def add_pairs(step):
+        total = own[step, pair_at].astype(jnp.float32)
+        for hop in range(1, half):
+            pair_copy(step, hop).wait_recv()
+            total = total + from_pair[step, hop - 1].astype(jnp.float32)
+        final[step] = total.astype(jnp.bfloat16)
+
+    def send_row(step):
+        add_pairs(step)
+        row_copy(step).start()
+
+    loop(1, sp_count, send_row)
+    add_pairs(0)
+    keep = pltpu.make_async_copy(final.at[0], result_ref.at[sp_at], own_sem)
+    keep.start()
+    keep.wait()
+
+    def finish(step):
+        mate_copy(step).wait_send()
+        for hop in range(1, half):
+            pair_copy(step, hop).wait_send()
+
+    loop(0, sp_count, finish)
+
+    def finish_rows(step):
+        row_arrival(step).wait_recv()
+        row_copy(step).wait_send()
+
+    loop(1, sp_count, finish_rows)
+
+
+def bring_back(partial, collective_id):
+    sp_count, half, sides, rows, width = partial.shape
+    tp_count = half * sides
+    sems = pltpu.SemaphoreType.DMA
+    return pl.pallas_call(
+        functools.partial(bring_kernel, sp_count, tp_count),
+        out_shape=jax.ShapeDtypeStruct((sp_count, rows, width), partial.dtype),
+        in_specs=[pl.BlockSpec(memory_space=pl.ANY)],
+        out_specs=pl.BlockSpec(memory_space=pl.ANY),
+        scratch_shapes=[
+            pltpu.VMEM((sp_count, half, rows, width), partial.dtype),
+            pltpu.VMEM((sp_count, half, rows, width), partial.dtype),
+            pltpu.VMEM((sp_count, max(1, half - 1), rows, width), partial.dtype),
+            pltpu.VMEM((sp_count, rows, width), partial.dtype),
+            sems((sp_count,)),
+            sems((sp_count,)),
+            sems((sp_count,)),
+            sems((sp_count, half)),
+            sems((sp_count, half)),
+            sems((sp_count,)),
+            sems((sp_count,)),
+            sems,
+        ],
+        compiler_params=pltpu.CompilerParams(collective_id=collective_id, has_side_effects=True),
+    )(partial)
 
 
 def from_behind(value, axis, steps):
@@ -12,10 +372,19 @@
     return lax.ppermute(value, axis, [(source, source + steps) for source in range(initial, last)])
 
 
-def slot_ranks(pair_ids, experts):
-    onehot = (pair_ids[..., None] == jnp.arange(experts, dtype=jnp.int32)).astype(jnp.int32)
-    ranks = jnp.cumsum(onehot, axis=-2) - 1
-    return jnp.sum(ranks * onehot, axis=-1)
+def slot_choice(ids, experts, capacity):
+    tokens, top_count = ids.shape
+    onehots = [ids[:, k : k + 1] == jnp.arange(experts, dtype=jnp.int32)[None, :] for k in range(top_count)]
+    named = sum(onehot.astype(jnp.bfloat16) for onehot in onehots)
+    order = jnp.arange(tokens, dtype=jnp.int32)
+    earlier = (order[None, :] < order[:, None]).astype(jnp.bfloat16)
+    ranks = jnp.dot(earlier, named, preferred_element_type=jnp.float32).astype(jnp.int32)
+    places = ranks + capacity * jnp.arange(experts, dtype=jnp.int32)[None, :]
+    slots = jnp.arange(experts * capacity, dtype=jnp.int32)[None, :]
+    return [
+        (jnp.sum(jnp.where(onehot, places, 0), axis=1, keepdims=True) == slots).astype(jnp.bfloat16)
+        for onehot in onehots
+    ]
 
 
 def expert_work(rows_in, cot_rows, gate_w, up_w, down_w):
@@ -46,6 +415,12 @@
         grads_pair, weights_pair, (((1, 2), (1, 2)), ((), ())), preferred_element_type=jnp.float32
     ).astype(jnp.bfloat16)
     return (gate_wgrad, up_wgrad, down_grad, back_rows)
+
+
+def pick(choice, rows):
+    return lax.dot_general(
+        choice, rows, (((0,), (0,)), ((), ())), preferred_element_type=jnp.float32
+    ).astype(jnp.bfloat16)
 
 
 def shards(
@@ -73,33 +448,19 @@
     inv_rms = lax.rsqrt(jnp.mean(inputs * inputs, axis=1, keepdims=True) + epsilon)
     scaled = inputs * inv_rms
     normed = (scaled * norm_gain[None, :]).astype(jnp.bfloat16)
-    group_ids = route_ids.reshape(tp_count, top_count * tok_rows)
-    group_slots = slot_ranks(group_ids, sp_count)
-    own_ids = lax.dynamic_index_in_dim(group_ids, tp_index, 0, keepdims=False)
-    own_slots = lax.dynamic_index_in_dim(group_slots, tp_index, 0, keepdims=False)
-    own_places = own_ids * capacity + own_slots
+    own_ids = lax.dynamic_slice_in_dim(route_ids, tp_index * tok_rows, tok_rows, 0)
     own_wts = lax.dynamic_slice_in_dim(route_wts, tp_index * tok_rows, tok_rows, 0)
-    own_weighted = (own_wts[:, :, None] * stream_cot.astype(jnp.float32)[:, None, :]).astype(
-        jnp.bfloat16
-    )
-    own_weighted = own_weighted.reshape(-1, model_width)
-    own_rows = jnp.repeat(normed, top_count, axis=0)
-    buffer_rows = (
-        jnp.zeros((sp_count * capacity, model_width), jnp.bfloat16).at[own_places].set(own_rows)
-    )
-    buffer_cot = (
-        jnp.zeros((sp_count * capacity, model_width), jnp.bfloat16).at[own_places].set(own_weighted)
-    )
-    buffer_rows = buffer_rows.reshape(sp_count, capacity, model_width)
-    buffer_cot = buffer_cot.reshape(sp_count, capacity, model_width)
-    landed_rows, landed_cot = (
-        lax.all_to_all(buffer_rows, "sp", split_axis=0, concat_axis=0, tiled=True),
-        lax.all_to_all(buffer_cot, "sp", split_axis=0, concat_axis=0, tiled=True),
-    )
-    arrived_rows, arrived_cot = (
-        lax.all_gather(landed_rows, "tp", axis=1, tiled=True),
-        lax.all_gather(landed_cot, "tp", axis=1, tiled=True),
-    )
+    choice = slot_choice(own_ids, sp_count, capacity)
+    chosen = sum(choice)
+    cot = stream_cot.astype(jnp.float32)
+    weighted = jnp.concatenate(
+        [(own_wts[:, k : k + 1] * cot).astype(jnp.bfloat16) for k in range(top_count)], axis=0
+    )
+    buffer_rows = pick(chosen, normed).reshape(sp_count, capacity, model_width)
+    buffer_cot = pick(jnp.concatenate(choice, axis=0), weighted).reshape(
+        sp_count, capacity, model_width
+    )
+    arrived_rows, arrived_cot = spread(sp_count, tp_count, [buffer_rows, buffer_cot], [], 1)
     gate_wgrad, up_wgrad, down_grad, back_rows = expert_work(
         arrived_rows.reshape(-1, model_width),
         arrived_cot.reshape(-1, model_width),
@@ -107,21 +468,22 @@
         w_up[0],
         w_down[0],
     )
-    back_rows = back_rows.reshape(sp_count, tp_count * capacity, model_width)
-    summed_back = lax.psum_scatter(
-        back_rows.astype(jnp.float32).astype(jnp.bfloat16), "tp", scatter_dimension=1, tiled=True
-    )
-    returned = lax.all_to_all(summed_back, "sp", split_axis=0, concat_axis=0, tiled=True)
-    picked = returned.reshape(sp_count * capacity, model_width)[own_places]
-    grad_normed = jnp.sum(
-        picked.astype(jnp.float32).reshape(tok_rows, top_count, model_width), axis=1
+    returned = bring_back(
+        back_rows.reshape(sp_count, tp_count // 2, 2, capacity, model_width), 2
+    )
+    grad_normed = jnp.dot(
+        chosen,
+        returned.reshape(sp_count * capacity, model_width),
+        preferred_element_type=jnp.float32,
     )
     q_term = grad_normed * norm_gain[None, :]
     stream_grad = (
         stream_cot.astype(jnp.float32)
         + inv_rms * (q_term - scaled * jnp.mean(q_term * scaled, axis=1, keepdims=True))
     ).astype(jnp.bfloat16)
-    group_grad = lax.all_gather(stream_grad, "tp", axis=0, tiled=True)
+    feature_blocks = stream_grad.reshape(tok_rows, sp_count, -1).transpose(1, 0, 2)
+    own_features, group_grad = spread(sp_count, tp_count, [feature_blocks], [stream_grad], 3)
+    group_grad = group_grad.reshape(-1, model_width)
     grad_mix = lax.dot_general(
         group_grad, out_proj, (((1,), (1,)), ((), ())), preferred_element_type=jnp.float32
     ).astype(jnp.bfloat16)
@@ -135,13 +497,12 @@
         + conv_taps[2][None, :] * conv_in[2:]
     )
     mixed = (conv_b.astype(jnp.float32) * conv_out).astype(jnp.bfloat16)
-    proj_grad = lax.psum_scatter(
-        lax.dot_general(
-            group_grad, mixed, (((0,), (0,)), ((), ())), preferred_element_type=jnp.float32
-        ),
-        "sp",
-        scatter_dimension=0,
-        tiled=True,
+    all_mixed = lax.all_gather(mixed, "sp", axis=0, tiled=True)
+    proj_grad = lax.dot_general(
+        own_features.reshape(all_mixed.shape[0], -1),
+        all_mixed,
+        (((0,), (0,)), ((), ())),
+        preferred_element_type=jnp.float32,
     )
     grad_b = (grad_mix.astype(jnp.float32) * conv_out).astype(jnp.bfloat16)
     rim_next = from_behind(jnp.stack([grad_mix[:2], conv_b[:2]]), "sp", -1)

time: 351 us -> 267 us (0.76)
  Pallas kernels: 0 us -> 167 us
  waiting for transfers between devices: 180 us -> 30.3 us
  blocking collectives: 72.9 us -> 0 us
  local copies, waits for them, and re-layouts: 21.9 us -> 4.29 us
  other arithmetic: 14.9 us -> 4.66 us
  starting transfers between devices: 10.9 us -> 6.22 us
  matrix products: 35.8 us -> 40.2 us
    pallas_call x0 -> x3, Pallas kernels: none -> 167 us  [the longest x2 115 us: spread(): pl.pallas_call(functools.partial(spread_kernel, sp_count, tp_count, len(e...]
    all_to_all x2 -> x0, blocking collectives: 72.9 us -> none  [the longest x1 38.6 us: shards(): lax.all_to_all(buffer_rows, 'sp', split_axis=0, concat_axis=0, tiled=True)]
    unnamed x6 -> x1, waiting for transfers between devices: 51.6 us -> 0.02 us
    reduce_scatter x1 -> x0, waiting for transfers between devices: 49.1 us -> none  [shards(): lax.psum_scatter(lax.dot_general(group_grad, mixed, (((0,), (0,)), ((), (...]
    all_to_all x1 -> x0, waiting for transfers between devices: 31 us -> none  [shards(): lax.all_to_all(summed_back, 'sp', split_axis=0, concat_axis=0, tiled=True)]
    all_gather x3 -> x1, waiting for transfers between devices: 46.3 us -> 29.1 us  [shards(): all_mixed = lax.all_gather(mixed, 'sp', axis=0, tiled=True)]
    unnamed x50 -> x48, local copies, waits for them, and re-layouts: 9.63 us -> 1.1 us
    dot_general x1 -> x5, matrix products: 2.11 us -> 10 us  [the longest x2 4.31 us: pick(): lax.dot_general(choice, rows, (((0,), (0,)), ((), ())), preferred_element...]
  transfers between devices with their start and end apart: 8 -> 3, of which waited for: 7 -> 2; matrix products, arithmetic and copies ran while one was open for 9% -> 15% of each run, Pallas kernels for 0% -> 62%
where the time goes in v1:
time: 267 us
  Pallas kernels  167 us (63%)
  matrix products  40.2 us (15%)
  waiting for transfers between devices  30.3 us (11%)
  between operations  14.4 us (5%)
  starting transfers between devices  6.22 us (2%)
  other arithmetic  4.66 us (2%)
  local copies, waits for them, and re-layouts  4.29 us (2%)
    pallas_call x2, Pallas kernels, spread(): pl.pallas_call(functools.partial(spread_kernel, sp_count, tp_count, len(e...  115 us
    pallas_call x1, Pallas kernels, bring_back(): pl.pallas_call(functools.partial(bring_kernel, sp_count, tp_count), out_s...  52 us
    all_gather x1, waiting for transfers between devices, shards(): all_mixed = lax.all_gather(mixed, 'sp', axis=0, tiled=True)  29.1 us
    ppermute x2, starting transfers between devices, from_behind(): lax.ppermute(value, axis, [(source, source + steps) for source in range(i...  6.19 us
    dot_general x1, matrix products, expert_work(): lax.dot_general(hidden, cot_rows, (((0,), (0,)), ((), ())), preferred_ele...  5.75 us
    dot_general x1, matrix products, expert_work(): lax.dot_general(rows_in, up_grad, (((0,), (0,)), ((), ())), preferred_ele...  5.54 us
  transfers between devices with their start and end apart: 3, of which 2 were waited for; matrix products, arithmetic and copies ran while one was open for 15% of the time, Pallas kernels for 62%

profile of v1, /device:TPU:0, one launch (start us, length us, event | category | flops | bytes accessed | tf_op | source)
XLA Modules:
  0.0 266.6 jit_solution(4826442758836514425)
XLA Ops:
  7.2 0.0 copy-start
  7.2 0.0 all-gather.2.cloned.1.call-start
  7.2 0.8 slice_bitcast_fusion.4
  8.1 4.9 %collective-permute-start = (bf16[2,2,256]{2,1,0:T(2,128)(2,1)S(1)}, bf16[2,2,256]{2,1,0:T(2,128)(2,1)S(1)}, u32[]{:S(2)}, u32[]{:S(2)}) collective-permute-start(bf16[2,2,256]{2,1,0:T(2,128)(2,1)S(1)} %pad_maximum_fusion.1), channel_id=1, source_target_pairs={{0,4},{4,8},{8,12},{12,16},{16,20},{20,24},{24,28},{1,5},{5,9},{9,... | collective-permute-start | bytes 6152 | tf_op jit(solution)/shard_map/ppermute | solution.py:372
  13.0 1.2 fusion.15
  14.2 0.7 constant_dynamic-slice_fusion.1
  14.9 0.7 constant_dynamic-slice_fusion
  15.6 0.1 select_reduce_fusion.1
  15.8 0.1 fusion.44
  15.9 2.7 %convolution_convert_fusion = bf16[320,2048]{1,0:T(8,128)(2,1)} fusion(bf16[128,2048]{1,0:T(8,128)(2,1)} %param.13, f32[2048]{0:T(1024)} %param.17, f32[128]{0:T(128)S(1)} %add_rsqrt_fusion, s32[128]{0:T(128)S(1)} %get-tuple-element.16, s32[128]{0:T(128)S(1)} %get-tuple-element.15), kind=kOutput, calls=%fused_computation.4 | convolution fusion | flops 169803776 | bytes 1844736 | tf_op jit(solution)/shard_map/dot_general | solution.py:421
  18.6 0.2 fusion.16
  18.9 1.6 convolution_convert_fusion.1
  20.5 76.2 %shard_map.180 = (bf16[8,4,40,2048]{3,2,1,0:T(8,128)(2,1)}, bf16[8,4,40,2048]{3,2,1,0:T(8,128)(2,1)}) custom-call(bf16[8,40,2048]{2,1,0:T(8,128)(2,1)} %bitcast.77, bf16[8,40,2048]{2,1,0:T(8,128)(2,1)} %bitcast.81), custom_call_target="tpu_custom_call" | custom-call | tf_op jit(solution)/shard_map/pallas_call | solution.py:204
  96.7 0.0 copy-start.11
  96.7 0.0 slice-start.2
  96.7 4.2 %fusion.22 = f32[1280,256]{1,0:T(8,128)S(1)} fusion(bf16[1280,2048]{1,0:T(8,128)(2,1)} %bitcast.88, bf16[1,2048,256]{2,1,0:T(8,128)(2,1)S(1)} %copy-done.10), kind=kOutput, calls=%fused_computation.40 | convolution fusion | flops 1342177280 | bytes 7602176 | tf_op jit(solution)/shard_map/dot_general | solution.py:391
  100.9 0.1 copy-done.11
  101.0 1.6 fusion.24
  102.6 0.0 copy-start.18
  102.6 0.1 slice-done.2
  102.8 0.4 slice-done.3
  103.2 2.1 multiply_convert_fusion.1
  105.3 0.0 copy-start.14
  105.3 4.7 %bitcast_convert_fusion = bf16[1280,2048]{1,0:T(8,128)(2,1)} fusion(bf16[2048,1,256]{2,0,1:T(8,128)(2,1)S(1)} %bitcast.101, bf16[2048,1,256]{2,0,1:T(8,128)(2,1)S(1)} %bitcast.100, bf16[1280,1,256]{2,0,1:T(8,128)(2,1)S(1)} %bitcast.103, bf16[1280,1,256]{2,0,1:T(8,128)(2,1)S(1)} %bitcast.102), kind=kOutput, calls=%fused_computation | convolution fusion | flops 2688679936 | bytes 8650752 | tf_op jit(solution)/shard_map/dot_general | solution.py:414
  110.0 52.0 %shard_map.181 = bf16[8,40,2048]{2,1,0:T(8,128)(2,1)} custom-call(bf16[8,2,2,40,2048]{4,3,2,1,0:T(8,128)(2,1)} %bitcast.76), custom_call_target="tpu_custom_call" | custom-call | tf_op jit(solution)/shard_map/pallas_call | solution.py:346
  162.1 0.0 copy-start.8
  162.1 1.9 fusion.12
  164.0 0.0 copy-start.4
  164.0 0.0 copy-start.5
  164.0 0.4 fusion.18.refs_1_
  164.4 1.0 copy.23
  165.4 0.0 copy-done.2
  165.4 38.3 %shard_map.182 = (bf16[8,4,128,256]{3,2,1,0:T(8,128)(2,1)}, bf16[4,128,2048]{2,1,0:T(8,128)(2,1)}) custom-call(bf16[8,128,256]{2,1,0:T(8,128)(2,1)} %bitcast.80, bf16[128,2048]{1,0:T(8,128)(2,1)} %copy-done.2), custom_call_target="tpu_custom_call" | custom-call | tf_op jit(solution)/shard_map/pallas_call | solution.py:204
  203.8 0.1 convert_multiply_fusion.7
  203.9 0.0 copy-start.6
  203.9 3.4 %fusion.33 = (bf16[512,256]{1,0:T(8,128)(2,1)}, f32[512,256]{1,0:T(8,128)S(1)}, bf16[512,256]{1,0:T(8,128)(2,1)S(1)}) fusion(f32[514,256]{1,0:T(8,128)S(1)} %convert_multiply_fusion.7, f32[256]{0:T(256)S(1)} %bitcast.84, f32[256]{0:T(256)S(1)} %bitcast.86, f32[256]{0:T(256)S(1)} %bitcast.82, bf16[512,2048]{1,0:T(8,128)(2,1)} %bitcast.99, ...), kind=kOutput, calls=%fused_computation.57 | convolution fusion | flops 538050560 | bytes 5770240 | tf_op jit(solution)/shard_map/dot_general | solution.py:487
  207.3 0.8 convert_multiply_fusion.4
  208.1 0.0 all-gather.2.cloned.1.call-update
  208.2 0.3 copy-done.15
  208.5 5.5 %convolution_bitcast_fusion.1 = f32[1,2048,256]{2,1,0:T(8,128)} fusion(bf16[1280,2048]{1,0:T(8,128)(2,1)} %bitcast.89, bf16[1280,256]{1,0:T(8,128)(2,1)S(1)} %copy-done.15), kind=kOutput, calls=%fused_computation.2 | convolution fusion | flops 1342177280 | bytes 7995392 | tf_op jit(solution)/shard_map/dot_general | solution.py:409
  214.0 5.7 %convolution_bitcast_fusion = f32[1,256,2048]{2,1,0:T(8,128)} fusion(bf16[1280,2048]{1,0:T(8,128)(2,1)} %bitcast.94, f32[1280,256]{1,0:T(8,128)S(1)} %copy-done.19, f32[1280,256]{1,0:T(8,128)S(1)} %copy-done.17), kind=kOutput, calls=%fused_computation.1 | convolution fusion | flops 1344143360 | bytes 9961472 | tf_op jit(solution)/shard_map/dot_general | solution.py:396
  219.8 1.3 collective-permute-start.1
  221.1 3.0 %convolution_bitcast_fusion.2 = f32[1,2048,256]{2,1,0:T(8,128)} fusion(bf16[1280,2048]{1,0:T(8,128)(2,1)S(1)} %bitcast.93, bf16[1280,256]{1,0:T(8,128)(2,1)S(1)} %copy-done.13), kind=kOutput, calls=%fused_computation.3 | convolution fusion | flops 1342177280 | bytes 7995392 | tf_op jit(solution)/shard_map/dot_general | solution.py:406
  224.1 1.1 collective-permute-done.1
  225.3 0.9 multiply_convert_fusion.4
  226.2 0.8 multiply_convert_fusion.5
  227.0 29.1 %all-gather.2.cloned.1.call-done = bf16[4096,256]{1,0:T(8,128)(2,1)} async-done(((bf16[512,256]{1,0:T(8,128)(2,1)}), bf16[4096,256]{1,0:T(8,128)(2,1)}) %all-gather.2.cloned.1.call-update) | async-done | bytes 2097168 | tf_op jit(solution)/shard_map/all_gather | solution.py:500
  256.1 3.7 %fusion.64 = f32[256,256]{1,0:T(8,128)} fusion(bf16[4096,256]{1,0:T(8,128)(2,1)} %bitcast.98, bf16[4096,256]{1,0:T(8,128)(2,1)} %all-gather.2.cloned.1.call-done), kind=kOutput, calls=%fused_computation.110 | convolution fusion | flops 536870912 | bytes 4456448 | tf_op jit(solution)/shard_map/dot_general | solution.py:501
  (49 shorter events, 0.1 us)
Async XLA Ops:
  7.2 95.5 %copy-start = (bf16[1,256,2048]{2,1,0:T(8,128)(2,1)S(1)}, bf16[1,256,2048]{2,1,0:T(8,128)(2,1)}, u32[]{:S(2)}) copy-start(bf16[1,256,2048]{2,1,0:T(8,128)(2,1)} %param.20) | copy-start | bytes 3145732
  7.2 11.4 %copy-start.3 = (bf16[128,2048]{1,0:T(8,128)(2,1)S(1)}, bf16[128,2048]{1,0:T(8,128)(2,1)}, u32[]{:S(2)}) copy-start(bf16[128,2048]{1,0:T(8,128)(2,1)} %param.14) | copy-start | bytes 1572868
  7.2 248.9 %all-gather.2.cloned.1.call-start = ((), (), s32[]{:S(2)}) async-start(), calls=%async_computation | async-start | bytes 2359296 | tf_op jit(solution)/shard_map/all_gather | solution.py:500
  8.1 195.7 %collective-permute-start = (bf16[2,2,256]{2,1,0:T(2,128)(2,1)S(1)}, bf16[2,2,256]{2,1,0:T(2,128)(2,1)S(1)}, u32[]{:S(2)}, u32[]{:S(2)}) collective-permute-start(bf16[2,2,256]{2,1,0:T(2,128)(2,1)S(1)} %pad_maximum_fusion.1), channel_id=1, source_target_pairs={{0,4},{4,8},{8,12},{12,16},{16,20},{20,24},{24,28},{1,5},{5,9},{9,... | collective-permute-start | bytes 6152 | tf_op jit(solution)/shard_map/ppermute | solution.py:372
  20.5 76.2 %copy-start.10 = (bf16[1,2048,256]{2,1,0:T(8,128)(2,1)S(1)}, bf16[1,2048,256]{2,1,0:T(8,128)(2,1)}, u32[]{:S(2)}) copy-start(bf16[1,2048,256]{2,1,0:T(8,128)(2,1)} %param.18) | copy-start | bytes 3145732
  96.7 4.2 %copy-start.9 = (bf16[8,4,40,2048]{3,2,1,0:T(8,128)(2,1)S(1)}, bf16[8,4,40,2048]{3,2,1,0:T(8,128)(2,1)}, u32[]{:S(2)}) copy-start(bf16[8,4,40,2048]{3,2,1,0:T(8,128)(2,1)} %get-tuple-element.11) | copy-start | bytes 15728644
  96.7 4.3 %copy-start.11 = (bf16[1,2048,256]{2,1,0:T(8,128)(2,1)S(1)}, bf16[1,2048,256]{2,1,0:T(8,128)(2,1)}, u32[]{:S(2)}) copy-start(bf16[1,2048,256]{2,1,0:T(8,128)(2,1)} %param.19) | copy-start | bytes 3145732
  96.7 6.1 %slice-start.2 = ((s8[5242880]{0:T(1024)(128)(4,1)}), s8[4194304]{0:T(1024)(128)(4,1)S(1)}, s32[]{:S(2)}) async-start(s8[5242880]{0:T(1024)(128)(4,1)} %bitcast.95), calls=%async_computation.3 | async-start | bytes 8388608
  101.0 1.6 copy-start.16
  101.0 2.1 slice-start.3
  102.6 2.6 copy-start.18
  105.3 4.7 %copy-start.12 = (bf16[1280,256]{1,0:T(8,128)(2,1)}, bf16[1280,256]{1,0:T(8,128)(2,1)S(1)}, u32[]{:S(2)}) copy-start(bf16[1280,256]{1,0:T(8,128)(2,1)S(1)} %get-tuple-element.22) | copy-start | bytes 1966084
  105.3 4.7 %copy-start.14 = (bf16[1280,256]{1,0:T(8,128)(2,1)}, bf16[1280,256]{1,0:T(8,128)(2,1)S(1)}, u32[]{:S(2)}) copy-start(bf16[1280,256]{1,0:T(8,128)(2,1)S(1)} %get-tuple-element.21) | copy-start | bytes 1966084
  110.0 52.1 %copy-start.1 = (bf16[128,2048]{1,0:T(8,128)(2,1)S(1)}, bf16[128,2048]{1,0:T(8,128)(2,1)}, u32[]{:S(2)}) copy-start(bf16[128,2048]{1,0:T(8,128)(2,1)} %param.13) | copy-start | bytes 1572868
  110.0 52.1 %copy-start.7 = (f32[2048]{0:T(1024)S(1)}, f32[2048]{0:T(1024)}, u32[]{:S(2)}) copy-start(f32[2048]{0:T(1024)} %param.17) | copy-start | bytes 24580
  162.1 2.4 copy-start.8
  164.0 39.8 %copy-start.4 = (bf16[512,256]{1,0:T(8,128)(2,1)S(1)}, bf16[512,256]{1,0:T(8,128)(2,1)}, u32[]{:S(2)}) copy-start(bf16[512,256]{1,0:T(8,128)(2,1)} %param.23) | copy-start | bytes 786436
  164.0 39.8 %copy-start.5 = (bf16[512,256]{1,0:T(8,128)(2,1)S(1)}, bf16[512,256]{1,0:T(8,128)(2,1)}, u32[]{:S(2)}) copy-start(bf16[512,256]{1,0:T(8,128)(2,1)} %param.24) | copy-start | bytes 786436
  164.4 1.0 copy-start.2
  203.9 3.4 %copy-start.6 = (bf16[512,256]{1,0:T(8,128)(2,1)S(1)}, bf16[512,256]{1,0:T(8,128)(2,1)}, u32[]{:S(2)}) copy-start(bf16[512,256]{1,0:T(8,128)(2,1)} %param.22) | copy-start | bytes 786436
  207.3 1.2 copy-start.15
  208.5 5.5 %copy-start.17 = (f32[1280,256]{1,0:T(8,128)S(1)}, f32[1280,256]{1,0:T(8,128)}, u32[]{:S(2)}) copy-start(f32[1280,256]{1,0:T(8,128)} %copy-done.16) | copy-start | bytes 3932164
  208.5 5.5 %copy-start.19 = (f32[1280,256]{1,0:T(8,128)S(1)}, f32[1280,256]{1,0:T(8,128)}, u32[]{:S(2)}) copy-start(f32[1280,256]{1,0:T(8,128)} %copy-done.18) | copy-start | bytes 3932164
  208.5 12.6 %slice-start = ((s8[5242880]{0:T(1024)(128)(4,1)}), s8[4194304]{0:T(1024)(128)(4,1)S(1)}, s32[]{:S(2)}) async-start(s8[5242880]{0:T(1024)(128)(4,1)} %bitcast.91), calls=%async_computation.1 | async-start | bytes 8388608
  214.0 7.1 %slice-start.1 = ((s8[5242880]{0:T(1024)(128)(4,1)}), s8[1048576]{0:T(1024)(128)(4,1)S(1)}, s32[]{:S(2)}) async-start(s8[5242880]{0:T(1024)(128)(4,1)} %bitcast.91), calls=%async_computation.2 | async-start | bytes 2097152
  214.0 7.1 %copy-start.13 = (bf16[1280,256]{1,0:T(8,128)(2,1)S(1)}, bf16[1280,256]{1,0:T(8,128)(2,1)}, u32[]{:S(2)}) copy-start(bf16[1280,256]{1,0:T(8,128)(2,1)} %copy-done.12) | copy-start | bytes 1966084
  219.8 5.5 %collective-permute-start.1 = (bf16[2,2,256]{2,1,0:T(2,128)(2,1)S(1)}, bf16[2,2,256]{2,1,0:T(2,128)(2,1)S(1)}, u32[]{:S(2)}, u32[]{:S(2)}) collective-permute-start(bf16[2,2,256]{2,1,0:T(2,128)(2,1)S(1)} %pad_maximum_fusion.2), channel_id=1, source_target_pairs={{4,0},{8,4},{12,8},{16,12},{20,16},{24,20},{28,24},{5,1},{9,5},{13... | collective-permute-start | bytes 6152 | tf_op jit(solution)/shard_map/ppermute | solution.py:372
Sparse Core Ops, SparseCore 0:
  208.3 47.7 all-gather.1

commit v2 on v1

--- a/solution.py
+++ b/solution.py
@@ -62,12 +62,31 @@
     lax.fori_loop(first, last, step, 0)
 
 
-def spread_kernel(sp_count, tp_count, exchanged, gathered, *refs):
+def spread_kernel(sp_count, tp_count, exchanged, gathered, shifted, lined, edged, *refs):
     count = exchanged + gathered
-    sources, results = refs[:count], refs[count : 2 * count]
-    own_sem, row_send, row_recv, pair_send, pair_recv, mate_send, mate_recv, last_send, last_recv = (
-        refs[2 * count :]
-    )
+    moved = len(shifted)
+    total = count + moved + lined
+    sources, results = refs[:count], refs[total : total + count]
+    shift_sources, shift_results = refs[count : count + moved], refs[total + count : total + count + moved]
+    line_source = refs[total - 1]
+    line_result = refs[2 * total - 1]
+    edge_result = refs[2 * total]
+    (
+        own_sem,
+        row_send,
+        row_recv,
+        pair_send,
+        pair_recv,
+        mate_send,
+        mate_recv,
+        last_send,
+        last_recv,
+        shift_send,
+        shift_recv,
+        line_send,
+        line_recv,
+        edge_sem,
+    ) = refs[2 * total + edged :]
     sp_at, tp_at = here()
     half = tp_count // 2
     mate = mate_of(tp_at)
@@ -148,7 +167,93 @@
             pair_copy(which, step, hop, own_block(which), origin_tp).wait_recv()
             last_copy(which, step, hop, origin_tp).start()
 
+    def shift_copy(index):
+        to = lax.rem(sp_at + sp_count + shifted[index], sp_count)
+        return remote(
+            shift_sources[index],
+            shift_results[index],
+            shift_send.at[index],
+            shift_recv.at[index],
+            to,
+            tp_at,
+        )
+
+    edge_rows = edge_result.shape[0] if edged else 0
+
+    def edge_copy():
+        return remote(
+            results[exchanged].at[0, pl.ds(0, edge_rows)],
+            edge_result,
+            edge_sem.at[0],
+            edge_sem.at[1],
+            origin(1),
+            tp_at,
+        )
+
+    depth = sp_count // 2
+    deep, lane = sp_at // 2, lax.rem(sp_at, 2)
+
+    def line_slot(where, side):
+        return line_result.at[where * 2 + side]
+
+    def line_copy(way, step):
+        toward = 1 - 2 * way
+        where = jnp.clip(deep - toward * step, 0, depth - 1)
+        return remote(
+            line_slot(where, lane),
+            line_slot(where, lane),
+            line_send.at[way, step],
+            line_recv.at[way, step + 1],
+            jnp.clip(deep + toward, 0, depth - 1) * 2 + lane,
+            tp_at,
+        )
+
+    def line_arrival(way, step):
+        toward = 1 - 2 * way
+        where = jnp.clip(deep - toward * step, 0, depth - 1)
+        return remote(
+            line_slot(where, lane),
+            line_slot(where, lane),
+            line_send.at[way, step],
+            line_recv.at[way, step],
+            jnp.clip(deep - toward, 0, depth - 1) * 2 + lane,
+            tp_at,
+        )
+
+    def line_mate(where, side):
+        return remote(
+            line_slot(where, side),
+            line_slot(where, side),
+            line_send.at[2, where],
+            line_recv.at[2, where],
+            deep * 2 + 1 - lane,
+            tp_at,
+        )
+
+    def reach(way):
+        return deep if way == 0 else depth - 1 - deep
+
+    def line_pass(way, step):
+        @pl.when(reach(1 - way) > 0)
+        def _():
+            line_copy(way, step).start()
+
+    def line_step(step):
+        for way in range(2):
+
+            @pl.when(step <= reach(way))
+            def _():
+                line_arrival(way, step).wait_recv()
+                line_pass(way, step)
+                toward = 1 - 2 * way
+                line_mate(jnp.clip(deep - toward * step, 0, depth - 1), lane).start()
+
     greet(sp_count, tp_count)
+    for index in range(moved):
+        shift_copy(index).start()
+    if lined:
+        line_own = pltpu.make_async_copy(line_source, line_slot(deep, lane), edge_sem.at[2])
+        line_own.start()
     for which in range(exchanged):
         loop(1, sp_count, lambda step: row_copy(which, step).start())
     locals_ = [
@@ -160,6 +265,11 @@
     for which in reversed(range(count)):
         pass_on(which, 0, own_block(which))
 
+    if lined:
+        line_own.wait()
+        for way in range(2):
+            line_pass(way, 0)
+        line_mate(deep, lane).start()
     for which in range(exchanged, count):
         pass_last(which, 0)
     for which in range(exchanged):
@@ -168,13 +278,18 @@
             row_arrival(which, step).wait_recv()
             pass_on(which, step, slot_of(which, step, tp_at))
             pass_last(which, step - 1)
+            if lined and which == 0:
+
+                @pl.when(lax.rem(step, 2) == 0)
+                def _():
+                    line_step(step // 2)
 
         loop(1, sp_count, relay)
         pass_last(which, sp_count - 1)
 
     for copy in locals_:
         copy.wait()
-    for which in range(count):
+    for which in reversed(range(count)):
         steps = sp_count if which < exchanged else 1
 
         def finish(step):
@@ -190,27 +305,68 @@
         loop(0, steps, finish)
         if which < exchanged:
             loop(1, sp_count, lambda step: row_copy(which, step).wait_send())
-
-
-def spread(sp_count, tp_count, exchanged, gathered, collective_id):
-    arrays = list(exchanged) + list(gathered)
-    count = len(arrays)
+        elif edged and which == exchanged:
+            edge_copy().start()
+
+    for index in range(moved):
+        shift_copy(index).wait()
+    if lined:
+        for way in range(2):
+
+            @pl.when(reach(1 - way) > 0)
+            def _():
+                loop(0, reach(way) + 1, lambda step: line_copy(way, step).wait_send())
+
+        def finish_line(where):
+            line_mate(where, lane).wait_send()
+            line_mate(where, 1 - lane).wait_recv()
+
+        loop(0, depth, finish_line)
+    if edged:
+        edge_copy().wait()
+
+
+def spread(sp_count, tp_count, exchanged, gathered, shifted, lined, edge_rows, collective_id):
+    arrays = exchanged + gathered + [value for value, _ in shifted] + lined
+    count = len(exchanged) + len(gathered)
     half = tp_count // 2
-    shapes = [
-        jax.ShapeDtypeStruct((sp_count, tp_count) + value.shape[1:], value.dtype)
-        for value in exchanged
-    ] + [jax.ShapeDtypeStruct((tp_count,) + value.shape, value.dtype) for value in gathered]
+    edged = 1 if edge_rows else 0
+    shapes = (
+        [(sp_count, tp_count) + value.shape[1:] for value in exchanged]
+        + [(tp_count,) + value.shape for value in gathered]
+        + [value.shape for value, _ in shifted]
+        + [(sp_count,) + value.shape for value in lined]
+    )
+    out_shape = [
+        jax.ShapeDtypeStruct(shape, value.dtype) for shape, value in zip(shapes, arrays)
+    ]
+    if edged:
+        out_shape.append(
+            jax.ShapeDtypeStruct((edge_rows, gathered[0].shape[1]), gathered[0].dtype)
+        )
     sems = pltpu.SemaphoreType.DMA
     return pl.pallas_call(
-        functools.partial(spread_kernel, sp_count, tp_count, len(exchanged), len(gathered)),
-        out_shape=tuple(shapes),
-        in_specs=[pl.BlockSpec(memory_space=pltpu.VMEM)] * count,
-        out_specs=tuple([pl.BlockSpec(memory_space=pl.ANY)] * count),
+        functools.partial(
+            spread_kernel,
+            sp_count,
+            tp_count,
+            len(exchanged),
+            len(gathered),
+            tuple(step for _, step in shifted),
+            len(lined),
+            edged,
+        ),
+        out_shape=tuple(out_shape),
+        in_specs=[pl.BlockSpec(memory_space=pltpu.VMEM)] * len(arrays),
+        out_specs=tuple([pl.BlockSpec(memory_space=pl.ANY)] * len(out_shape)),
         scratch_shapes=[sems((count,))]
         + [sems((count, sp_count))] * 2
         + [sems((count, sp_count, half))] * 2
         + [sems((count, sp_count))] * 2
-        + [sems((count, sp_count, half))] * 2,
+        + [sems((count, sp_count, half))] * 2
+        + [sems((max(1, len(shifted)),))] * 2
+        + [sems((3, sp_count // 2 + 1))] * 2
+        + [sems((3,))],
         compiler_params=pltpu.CompilerParams(collective_id=collective_id, has_side_effects=True),
     )(*arrays)
 
@@ -364,12 +520,6 @@
         ],
         compiler_params=pltpu.CompilerParams(collective_id=collective_id, has_side_effects=True),
     )(partial)
-
-
-def from_behind(value, axis, steps):
-    count = lax.axis_size(axis)
-    initial, last = (max(0, -steps), min(count, count - steps))
-    return lax.ppermute(value, axis, [(source, source + steps) for source in range(initial, last)])
 
 
 def slot_choice(ids, experts, capacity):
@@ -460,7 +610,17 @@
     buffer_cot = pick(jnp.concatenate(choice, axis=0), weighted).reshape(
         sp_count, capacity, model_width
     )
-    arrived_rows, arrived_cot = spread(sp_count, tp_count, [buffer_rows, buffer_cot], [], 1)
+    edge_rows = 8
+    arrived_rows, arrived_cot, c_before, h_before, b_after = spread(
+        sp_count,
+        tp_count,
+        [buffer_rows, buffer_cot],
+        [],
+        [(conv_c[-edge_rows:], 1), (conv_h[-edge_rows:], 1), (conv_b[:edge_rows], -1)],
+        [],
+        0,
+        1,
+    )
     gate_wgrad, up_wgrad, down_grad, back_rows = expert_work(
         arrived_rows.reshape(-1, model_width),
         arrived_cot.reshape(-1, model_width),
@@ -482,22 +642,26 @@
         + inv_rms * (q_term - scaled * jnp.mean(q_term * scaled, axis=1, keepdims=True))
     ).astype(jnp.bfloat16)
     feature_blocks = stream_grad.reshape(tok_rows, sp_count, -1).transpose(1, 0, 2)
-    own_features, group_grad = spread(sp_count, tp_count, [feature_blocks], [stream_grad], 3)
+    rim = conv_taps.shape[0] - 1
+    has_before = lax.axis_index("sp") > 0
+    gate_ext = jnp.concatenate([c_before[-rim:], conv_c], axis=0).astype(jnp.float32)
+    value_ext = jnp.concatenate([h_before[-rim:], conv_h], axis=0).astype(jnp.float32)
+    inside = has_before | (jnp.arange(gate_ext.shape[0])[:, None] >= rim)
+    conv_in = jnp.where(inside, gate_ext * value_ext, 0.0)
+    conv_out = (
+        conv_taps[0][None, :] * conv_in[:-2]
+        + conv_taps[1][None, :] * conv_in[1:-1]
+        + conv_taps[2][None, :] * conv_in[2:]
+    )
+    mixed = (conv_b.astype(jnp.float32) * conv_out).astype(jnp.bfloat16)
+    own_features, group_grad, all_mixed, edge_grad = spread(
+        sp_count, tp_count, [feature_blocks], [stream_grad], [], [mixed], edge_rows, 3
+    )
     group_grad = group_grad.reshape(-1, model_width)
     grad_mix = lax.dot_general(
         group_grad, out_proj, (((1,), (1,)), ((), ())), preferred_element_type=jnp.float32
     ).astype(jnp.bfloat16)
-    rim_prev = from_behind(jnp.stack([conv_c[-2:], conv_h[-2:]]), "sp", 1)
-    gate_ext = jnp.concatenate([rim_prev[0], conv_c], axis=0).astype(jnp.float32)
-    value_ext = jnp.concatenate([rim_prev[1], conv_h], axis=0).astype(jnp.float32)
-    conv_in = gate_ext * value_ext
-    conv_out = (
-        conv_taps[0][None, :] * conv_in[:-2]
-        + conv_taps[1][None, :] * conv_in[1:-1]
-        + conv_taps[2][None, :] * conv_in[2:]
-    )
-    mixed = (conv_b.astype(jnp.float32) * conv_out).astype(jnp.bfloat16)
-    all_mixed = lax.all_gather(mixed, "sp", axis=0, tiled=True)
+    all_mixed = all_mixed.reshape(-1, all_mixed.shape[-1])
     proj_grad = lax.dot_general(
         own_features.reshape(all_mixed.shape[0], -1),
         all_mixed,
@@ -505,9 +669,13 @@
         preferred_element_type=jnp.float32,
     )
     grad_b = (grad_mix.astype(jnp.float32) * conv_out).astype(jnp.bfloat16)
-    rim_next = from_behind(jnp.stack([grad_mix[:2], conv_b[:2]]), "sp", -1)
+    edge_mix = lax.dot_general(
+        edge_grad, out_proj, (((1,), (1,)), ((), ())), preferred_element_type=jnp.float32
+    ).astype(jnp.bfloat16)
     conv_grad = grad_mix.astype(jnp.float32) * conv_b.astype(jnp.float32)
-    next_grad = rim_next[0].astype(jnp.float32) * rim_next[1].astype(jnp.float32)
+    next_grad = edge_mix.astype(jnp.float32) * b_after.astype(jnp.float32)
+    has_after = lax.axis_index("sp") < sp_count - 1
+    next_grad = jnp.where(has_after, next_grad, 0.0)[:rim]
     grad_ext = jnp.concatenate([conv_grad, next_grad], axis=0)
     grad_in = (
         conv_taps[2][None, :] * grad_ext[:-2]

time: 267 us -> 227 us (0.85)
  waiting for transfers between devices: 30.3 us -> 0 us
  between operations: 14.4 us -> 0.93 us
  Pallas kernels: 167 us -> 178 us
  matrix products: 40.2 us -> 32.7 us
  starting transfers between devices: 6.22 us -> 0 us
  local copies, waits for them, and re-layouts: 4.29 us -> 8.6 us
    all_gather x1 -> x0, waiting for transfers between devices: 29.1 us -> none  [shards(): all_mixed = lax.all_gather(mixed, 'sp', axis=0, tiled=True)]
    pallas_call x2, Pallas kernels: 115 us -> 126 us  [spread(): pl.pallas_call(functools.partial(spread_kernel, sp_count, tp_count, len(e...]
    ppermute x2 -> x0, starting transfers between devices: 6.19 us -> none  [from_behind(): lax.ppermute(value, axis, [(source, source + steps) for source in range(i...]
    slice x0 -> x5, local copies, waits for them, and re-layouts: none -> 5.32 us  [the longest x1 1.31 us: shards(): conv_c[-edge_rows:]]
    dot_general x1, matrix products: 5.75 us -> 2.93 us  [expert_work(): lax.dot_general(hidden, cot_rows, (((0,), (0,)), ((), ())), preferred_ele...]
  transfers between devices with their start and end apart: 3 -> 0, of which waited for: 2 -> 0; matrix products, arithmetic and copies ran while one was open for 15% -> 0% of each run, Pallas kernels for 62% -> 0%
where the time goes in v2:
time: 227 us
  Pallas kernels  178 us (78%)
  matrix products  32.7 us (14%)
  local copies, waits for them, and re-layouts  8.6 us (4%)
  other arithmetic  6.52 us (3%)
    pallas_call x2, Pallas kernels, spread(): pl.pallas_call(functools.partial(spread_kernel, sp_count, tp_count, len(e...  126 us
    pallas_call x1, Pallas kernels, bring_back(): pl.pallas_call(functools.partial(bring_kernel, sp_count, tp_count), out_s...  52.3 us
    dot_general x1, matrix products, expert_work(): lax.dot_general(grads_pair, weights_pair, (((1, 2), (1, 2)), ((), ())), p...  4.69 us

profile of v2, /device:TPU:0, one launch (start us, length us, event | category | flops | bytes accessed | tf_op | source)
XLA Modules:
  0.0 226.6 jit_solution(7887577056137785519)
XLA Ops:
  0.6 0.0 copy-start
  0.7 1.3 fusion.16
  2.0 0.7 constant_dynamic-slice_fusion.1
  2.7 0.1 select_reduce_fusion.1
  2.8 0.7 constant_dynamic-slice_fusion
  3.6 0.8 fusion.64
  4.4 1.3 slice.63.refs_4_
  5.6 1.3 slice.61.refs_2_
  6.9 1.3 slice.62.refs_3_
  8.2 0.1 fusion.44
  8.3 1.3 fusion.17
  9.6 0.0 copy-start.1
  9.6 0.0 copy-start.9
  9.6 1.6 convolution_convert_fusion.1
  11.2 0.0 copy-done.1
  11.2 0.0 copy-done.9
  11.2 1.7 convolution_convert_fusion
  12.9 78.3 %shard_map.180 = (bf16[8,4,40,2048]{3,2,1,0:T(8,128)(2,1)}, bf16[8,4,40,2048]{3,2,1,0:T(8,128)(2,1)}, bf16[8,256]{1,0:T(8,128)(2,1)}, bf16[8,256]{1,0:T(8,128)(2,1)}, bf16[8,256]{1,0:T(8,128)(2,1)}) custom-call(bf16[8,40,2048]{2,1,0:T(8,128)(2,1)} %bitcast.66, bf16[8,40,2048]{2,1,0:T(8,128)(2,1)} %bitcast.71, bf16[8,256]{1,0:T(8,128)(2,1)} %slice.61.refs_2_, ...), custom_call_target="tpu_custom_call" | custom-call | tf_op jit(solution)/shard_map/pallas_call | solution.py:348
  91.2 0.0 copy-start.11
  91.2 0.8 slice.65
  92.0 0.7 slice.66
  92.7 0.2 multiply_select_fusion
  92.9 0.0 slice-start
  92.9 0.9 fusion.33
  93.8 4.5 %fusion.23 = f32[1280,256]{1,0:T(8,128)S(1)} fusion(bf16[1280,2048]{1,0:T(8,128)(2,1)} %bitcast.78, bf16[1,2048,256]{2,1,0:T(8,128)(2,1)S(1)} %copy-done.11), kind=kOutput, calls=%fused_computation.41 | convolution fusion | flops 1342177280 | bytes 7602176 | tf_op jit(solution)/shard_map/dot_general | solution.py:541
  98.3 0.0 slice-start.3
  98.3 1.5 fusion.25
  99.9 2.1 multiply_convert_fusion.1
  102.0 2.9 %convolution_bitcast_fusion = f32[1,256,2048]{2,1,0:T(8,128)} fusion(bf16[1280,2048]{1,0:T(8,128)(2,1)S(1)} %bitcast.87, f32[1280,256]{1,0:T(8,128)S(1)} %fusion.25, f32[1280,256]{1,0:T(8,128)S(1)} %fusion.23), kind=kOutput, calls=%fused_computation.1 | convolution fusion | flops 1344143360 | bytes 9961472 | tf_op jit(solution)/shard_map/dot_general | solution.py:546
  104.9 3.0 %convolution_bitcast_fusion.1 = f32[1,2048,256]{2,1,0:T(8,128)} fusion(bf16[1280,2048]{1,0:T(8,128)(2,1)S(1)} %bitcast.82, bf16[1280,256]{1,0:T(8,128)(2,1)S(1)} %get-tuple-element.31), kind=kOutput, calls=%fused_computation.2 | convolution fusion | flops 1342177280 | bytes 7995392 | tf_op jit(solution)/shard_map/dot_general | solution.py:559
  107.9 3.0 %convolution_bitcast_fusion.2 = f32[1,2048,256]{2,1,0:T(8,128)} fusion(bf16[1280,2048]{1,0:T(8,128)(2,1)S(1)} %bitcast.83, bf16[1280,256]{1,0:T(8,128)(2,1)S(1)} %get-tuple-element.32), kind=kOutput, calls=%fused_computation.3 | convolution fusion | flops 1342177280 | bytes 7995392 | tf_op jit(solution)/shard_map/dot_general | solution.py:556
  110.9 4.7 %bitcast_convert_fusion = bf16[1280,2048]{1,0:T(8,128)(2,1)} fusion(bf16[2048,1,256]{2,0,1:T(8,128)(2,1)S(1)} %bitcast.91, bf16[2048,1,256]{2,0,1:T(8,128)(2,1)S(1)} %bitcast.90, bf16[1280,1,256]{2,0,1:T(8,128)(2,1)S(1)} %bitcast.92, bf16[1280,1,256]{2,0,1:T(8,128)(2,1)S(1)} %bitcast.93), kind=kOutput, calls=%fused_computation | convolution fusion | flops 2688679936 | bytes 8650752 | tf_op jit(solution)/shard_map/dot_general | solution.py:564
  115.6 52.3 %shard_map.181 = bf16[8,40,2048]{2,1,0:T(8,128)(2,1)} custom-call(bf16[8,2,2,40,2048]{4,3,2,1,0:T(8,128)(2,1)} %bitcast.65), custom_call_target="tpu_custom_call" | custom-call | tf_op jit(solution)/shard_map/pallas_call | solution.py:502
  167.9 0.0 copy-start.5
  167.9 2.0 fusion.13
  169.9 0.0 copy-done.5
  169.9 0.4 fusion.19.refs_1_
  170.3 0.9 copy.23
  171.2 0.1 copy-done.2
  171.3 47.2 %shard_map.182 = (bf16[8,4,128,256]{3,2,1,0:T(8,128)(2,1)}, bf16[4,128,2048]{2,1,0:T(8,128)(2,1)}, bf16[8,512,256]{2,1,0:T(8,128)(2,1)}, bf16[8,2048]{1,0:T(8,128)(2,1)}) custom-call(bf16[8,128,256]{2,1,0:T(8,128)(2,1)} %bitcast.70, bf16[128,2048]{1,0:T(8,128)(2,1)} %copy-done.2, bf16[512,256]{1,0:T(8,128)(2,1)} %get-tuple-element.29.refs_2_), custom_call_target="tpu_custom_call" | custom-call | tf_op jit(solution)/shard_map/pallas_call | solution.py:348
  218.5 0.0 copy-start.3
  218.5 3.8 %fusion.65 = f32[256,256]{1,0:T(8,128)} fusion(bf16[4096,256]{1,0:T(8,128)(2,1)} %bitcast.88, bf16[4096,256]{1,0:T(8,128)(2,1)} %bitcast.89), kind=kOutput, calls=%fused_computation.105 | convolution fusion | flops 536870912 | bytes 4456448 | tf_op jit(solution)/shard_map/dot_general | solution.py:665
  222.4 0.0 copy-done.3
  222.4 0.4 fusion.66
  222.7 1.5 convert_multiply_fusion.4
  224.2 0.7 multiply_select_fusion.1
  224.9 0.9 multiply_convert_fusion.4
  225.8 0.8 multiply_convert_fusion.5
  (29 shorter events, 0.1 us)
Async XLA Ops:
  0.6 99.3 %copy-start = (bf16[1,256,2048]{2,1,0:T(8,128)(2,1)S(1)}, bf16[1,256,2048]{2,1,0:T(8,128)(2,1)}, u32[]{:S(2)}) copy-start(bf16[1,256,2048]{2,1,0:T(8,128)(2,1)} %param.20) | copy-start | bytes 3145732
  9.6 1.6 copy-start.1
  9.6 1.6 copy-start.9
  11.2 81.4 %copy-start.6 = (bf16[512,256]{1,0:T(8,128)(2,1)S(1)}, bf16[512,256]{1,0:T(8,128)(2,1)}, u32[]{:S(2)}) copy-start(bf16[512,256]{1,0:T(8,128)(2,1)} %param.23) | copy-start | bytes 786436
  11.2 81.4 %copy-start.7 = (bf16[512,256]{1,0:T(8,128)(2,1)S(1)}, bf16[512,256]{1,0:T(8,128)(2,1)}, u32[]{:S(2)}) copy-start(bf16[512,256]{1,0:T(8,128)(2,1)} %param.24) | copy-start | bytes 786436
  12.9 79.9 %copy-start.8 = (bf16[512,256]{1,0:T(8,128)(2,1)S(1)}, bf16[512,256]{1,0:T(8,128)(2,1)}, u32[]{:S(2)}) copy-start(bf16[512,256]{1,0:T(8,128)(2,1)} %param.22) | copy-start | bytes 786436
  91.2 2.6 %copy-start.11 = (bf16[1,2048,256]{2,1,0:T(8,128)(2,1)S(1)}, bf16[1,2048,256]{2,1,0:T(8,128)(2,1)}, u32[]{:S(2)}) copy-start(bf16[1,2048,256]{2,1,0:T(8,128)(2,1)} %param.18) | copy-start | bytes 3145732
  92.9 5.4 %slice-start = ((s8[5242880]{0:T(1024)(128)(4,1)}), s8[4194304]{0:T(1024)(128)(4,1)S(1)}, s32[]{:S(2)}) async-start(s8[5242880]{0:T(1024)(128)(4,1)} %bitcast.79), calls=%async_computation | async-start | bytes 8388608
  93.8 4.5 %slice-start.1 = ((s8[5242880]{0:T(1024)(128)(4,1)}), s8[1048576]{0:T(1024)(128)(4,1)S(1)}, s32[]{:S(2)}) async-start(s8[5242880]{0:T(1024)(128)(4,1)} %bitcast.79), calls=%async_computation.1 | async-start | bytes 2097152
  93.8 4.5 %copy-start.12 = (bf16[1,2048,256]{2,1,0:T(8,128)(2,1)S(1)}, bf16[1,2048,256]{2,1,0:T(8,128)(2,1)}, u32[]{:S(2)}) copy-start(bf16[1,2048,256]{2,1,0:T(8,128)(2,1)} %param.19) | copy-start | bytes 3145732
  93.8 6.1 %slice-start.2 = ((s8[5242880]{0:T(1024)(128)(4,1)}), s8[4194304]{0:T(1024)(128)(4,1)S(1)}, s32[]{:S(2)}) async-start(s8[5242880]{0:T(1024)(128)(4,1)} %bitcast.84), calls=%async_computation.2 | async-start | bytes 8388608
  98.3 1.6 slice-start.3
  167.9 2.0 copy-start.5
  170.3 1.0 copy-start.2
  218.5 3.9 %copy-start.3 = (bf16[256,2048]{1,0:T(8,128)(2,1)S(1)}, bf16[256,2048]{1,0:T(8,128)(2,1)}, u32[]{:S(2)}) copy-start(bf16[256,2048]{1,0:T(8,128)(2,1)} %param.21) | copy-start | bytes 3145732
  218.5 3.8 %copy-start.10 = (bf16[8,2048]{1,0:T(8,128)(2,1)S(1)}, bf16[8,2048]{1,0:T(8,128)(2,1)}, u32[]{:S(2)}) copy-start(bf16[8,2048]{1,0:T(8,128)(2,1)} %get-tuple-element.23) | copy-start | bytes 98308
  218.5 4.2 %copy-start.4 = (bf16[4,128,2048]{2,1,0:T(8,128)(2,1)S(1)}, bf16[4,128,2048]{2,1,0:T(8,128)(2,1)}, u32[]{:S(2)}) copy-start(bf16[4,128,2048]{2,1,0:T(8,128)(2,1)} %get-tuple-element.22) | copy-start | bytes 6291460

commit v3 on v2

--- a/solution.py
+++ b/solution.py
@@ -37,6 +37,15 @@
 
 def pair_peer(tp_at, step, half):
     return lax.rem(tp_at // 2 + step, half) * 2 + lax.rem(tp_at, 2)
+
+
+def partner(at, step, count):
+    other = lax.rem(count - step, count)
+    total, bit = 0, 1
+    while bit < count:
+        total = total + bit * lax.rem(at // bit + other // bit, 2)
+        bit *= 2
+    return total
 
 
 def mate_of(tp_at):
@@ -92,7 +101,7 @@
     mate = mate_of(tp_at)
 
     def origin(step):
-        return lax.rem(sp_at + sp_count - step, sp_count)
+        return partner(sp_at, step, sp_count)
 
     def slot_of(which, step, tp_from):
         if which < exchanged:
@@ -103,7 +112,7 @@
         return sources[which].at[sp_at] if which < exchanged else sources[which]
 
     def row_copy(which, step):
-        to = lax.rem(sp_at + step, sp_count)
+        to = origin(step)
         return remote(
             sources[which].at[to],
             results[which].at[sp_at, tp_at],
@@ -169,8 +178,10 @@
 
     def shift_copy(index):
         to = lax.rem(sp_at + sp_count + shifted[index], sp_count)
-        return remote(
-            shift_sources[index],
+        rows = shift_results[index].shape[0]
+        first = shift_sources[index].shape[0] - rows if shifted[index] > 0 else 0
+        return remote(
+            shift_sources[index].at[pl.ds(first, rows)],
             shift_results[index],
             shift_send.at[index],
             shift_recv.at[index],
@@ -186,7 +197,7 @@
             edge_result,
             edge_sem.at[0],
             edge_sem.at[1],
-            origin(1),
+            lax.rem(sp_at + sp_count - 1, sp_count),
             tp_at,
         )
 
@@ -274,18 +285,25 @@
         pass_last(which, 0)
     for which in range(exchanged):
 
-        def relay(step):
+        def step_at(place):
+            return lax.rem(place + sp_count - 3, sp_count - 1) + 1
+
+        def relay(step, before):
             row_arrival(which, step).wait_recv()
             pass_on(which, step, slot_of(which, step, tp_at))
-            pass_last(which, step - 1)
+            pass_last(which, before)
+
+        def relay_at(place):
+            relay(step_at(place), step_at(place - 1))
             if lined and which == 0:
 
-                @pl.when(lax.rem(step, 2) == 0)
+                @pl.when(lax.rem(place, 2) == 0)
                 def _():
-                    line_step(step // 2)
-
-        loop(1, sp_count, relay)
-        pass_last(which, sp_count - 1)
+                    line_step(place // 2)
+
+        relay(sp_count - 1, 0)
+        loop(2, sp_count, relay_at)
+        pass_last(which, sp_count - 2)
 
     for copy in locals_:
         copy.wait()
@@ -330,11 +348,11 @@
     arrays = exchanged + gathered + [value for value, _ in shifted] + lined
     count = len(exchanged) + len(gathered)
     half = tp_count // 2
-    edged = 1 if edge_rows else 0
+    edged = 1 if edge_rows and gathered else 0
     shapes = (
         [(sp_count, tp_count) + value.shape[1:] for value in exchanged]
         + [(tp_count,) + value.shape for value in gathered]
-        + [value.shape for value, _ in shifted]
+        + [(edge_rows,) + value.shape[1:] for value, _ in shifted]
         + [(sp_count,) + value.shape for value in lined]
     )
     out_shape = [
@@ -357,7 +375,9 @@
             edged,
         ),
         out_shape=tuple(out_shape),
-        in_specs=[pl.BlockSpec(memory_space=pltpu.VMEM)] * len(arrays),
+        in_specs=[pl.BlockSpec(memory_space=pltpu.VMEM)] * count
+        + [pl.BlockSpec(memory_space=pl.ANY)] * len(shifted)
+        + [pl.BlockSpec(memory_space=pltpu.VMEM)] * len(lined),
         out_specs=tuple([pl.BlockSpec(memory_space=pl.ANY)] * len(out_shape)),
         scratch_shapes=[sems((count,))]
         + [sems((count, sp_count))] * 2
@@ -395,7 +415,7 @@
     mate = mate_of(tp_at)
 
     def target(step):
-        return lax.rem(sp_at + step, sp_count)
+        return partner(sp_at, step, sp_count)
 
     def load(step):
         return pltpu.make_async_copy(
@@ -433,7 +453,7 @@
         )
 
     def row_arrival(step):
-        came = lax.rem(sp_at + sp_count - step, sp_count)
+        came = target(step)
         return remote(
             final.at[step],
             result_ref.at[came],
@@ -616,9 +636,9 @@
         tp_count,
         [buffer_rows, buffer_cot],
         [],
-        [(conv_c[-edge_rows:], 1), (conv_h[-edge_rows:], 1), (conv_b[:edge_rows], -1)],
+        [(conv_c, 1), (conv_h, 1), (conv_b, -1)],
         [],
-        0,
+        edge_rows,
         1,
     )
     gate_wgrad, up_wgrad, down_grad, back_rows = expert_work(

time: 227 us -> 227 us (level)
  Pallas kernels: 178 us -> 182 us
  local copies, waits for them, and re-layouts: 8.6 us -> 5.03 us
    pallas_call x2, Pallas kernels: 126 us -> 140 us  [spread(): pl.pallas_call(functools.partial(spread_kernel, sp_count, tp_count, len(e...]
    pallas_call x1, Pallas kernels: 52.3 us -> 41.7 us  [bring_back(): pl.pallas_call(functools.partial(bring_kernel, sp_count, tp_count), out_s...]
    slice x3 -> x0, local copies, waits for them, and re-layouts: 3.87 us -> none  [the longest x1 1.31 us: shards(): conv_c[-edge_rows:]]
where the time goes in v3:
time: 227 us
  Pallas kernels  182 us (80%)
  matrix products  32.8 us (14%)
  other arithmetic  6.51 us (3%)
  local copies, waits for them, and re-layouts  5.03 us (2%)
    pallas_call x2, Pallas kernels, spread(): pl.pallas_call(functools.partial(spread_kernel, sp_count, tp_count, len(e...  140 us
    pallas_call x1, Pallas kernels, bring_back(): pl.pallas_call(functools.partial(bring_kernel, sp_count, tp_count), out_s...  41.7 us
    dot_general x1, matrix products, expert_work(): lax.dot_general(grads_pair, weights_pair, (((1, 2), (1, 2)), ((), ())), p...  4.69 us
    dot_general x1, matrix products, expert_work(): gate_pre = jnp.dot(rows_in, gate_w, preferred_element_type=jnp.float32)  4.59 us

profile of v3, /device:TPU:0, one launch (start us, length us, event | category | flops | bytes accessed | tf_op | source)
XLA Modules:
  0.0 226.8 jit_solution(1069940804605382606)
XLA Ops:
  0.6 0.0 copy-start
  0.7 1.3 fusion.16
  2.0 0.7 constant_dynamic-slice_fusion.1
  2.7 0.1 select_reduce_fusion.1
  2.8 0.7 constant_dynamic-slice_fusion
  3.6 0.8 fusion.64
  4.4 0.1 fusion.44
  4.5 1.3 fusion.17
  5.7 0.0 copy-start.1
  5.8 0.0 copy-start.9
  5.8 1.6 convolution_convert_fusion.1
  7.4 0.0 copy-done.1
  7.4 0.0 copy-done.9
  7.4 1.7 convolution_convert_fusion
  9.0 94.7 %shard_map.180 = (bf16[8,4,40,2048]{3,2,1,0:T(8,128)(2,1)}, bf16[8,4,40,2048]{3,2,1,0:T(8,128)(2,1)}, bf16[8,256]{1,0:T(8,128)(2,1)}, bf16[8,256]{1,0:T(8,128)(2,1)}, bf16[8,256]{1,0:T(8,128)(2,1)}) custom-call(bf16[8,40,2048]{2,1,0:T(8,128)(2,1)} %bitcast.66, bf16[8,40,2048]{2,1,0:T(8,128)(2,1)} %bitcast.71, bf16[512,256]{1,0:T(8,128)(2,1)} %refs_2_.1, ...), custom_call_target="tpu_custom_call" | custom-call | tf_op jit(solution)/shard_map/pallas_call | solution.py:366
  103.8 0.0 copy-start.11
  103.8 0.8 slice.53
  104.6 0.7 slice.54
  105.2 0.0 copy-done.4
  105.2 0.2 multiply_select_fusion
  105.4 0.0 slice-start
  105.4 0.0 slice-start.2
  105.4 0.9 fusion.33
  106.4 4.6 %fusion.23 = f32[1280,256]{1,0:T(8,128)S(1)} fusion(bf16[1280,2048]{1,0:T(8,128)(2,1)} %bitcast.78, bf16[1,2048,256]{2,1,0:T(8,128)(2,1)S(1)} %copy-done.11), kind=kOutput, calls=%fused_computation.41 | convolution fusion | flops 1342177280 | bytes 7602176 | tf_op jit(solution)/shard_map/dot_general | solution.py:561
  111.0 0.3 slice-done.1
  111.3 1.5 fusion.25
  112.9 2.1 multiply_convert_fusion.1
  114.9 2.9 %convolution_bitcast_fusion = f32[1,256,2048]{2,1,0:T(8,128)} fusion(bf16[1280,2048]{1,0:T(8,128)(2,1)S(1)} %bitcast.87, f32[1280,256]{1,0:T(8,128)S(1)} %fusion.25, f32[1280,256]{1,0:T(8,128)S(1)} %fusion.23), kind=kOutput, calls=%fused_computation.1 | convolution fusion | flops 1344143360 | bytes 9961472 | tf_op jit(solution)/shard_map/dot_general | solution.py:566
  117.9 3.0 %convolution_bitcast_fusion.1 = f32[1,2048,256]{2,1,0:T(8,128)} fusion(bf16[1280,2048]{1,0:T(8,128)(2,1)S(1)} %bitcast.82, bf16[1280,256]{1,0:T(8,128)(2,1)S(1)} %get-tuple-element.31), kind=kOutput, calls=%fused_computation.2 | convolution fusion | flops 1342177280 | bytes 7995392 | tf_op jit(solution)/shard_map/dot_general | solution.py:579
  120.9 3.0 %convolution_bitcast_fusion.2 = f32[1,2048,256]{2,1,0:T(8,128)} fusion(bf16[1280,2048]{1,0:T(8,128)(2,1)S(1)} %bitcast.83, bf16[1280,256]{1,0:T(8,128)(2,1)S(1)} %get-tuple-element.32), kind=kOutput, calls=%fused_computation.3 | convolution fusion | flops 1342177280 | bytes 7995392 | tf_op jit(solution)/shard_map/dot_general | solution.py:576
  123.8 4.7 %bitcast_convert_fusion = bf16[1280,2048]{1,0:T(8,128)(2,1)} fusion(bf16[2048,1,256]{2,0,1:T(8,128)(2,1)S(1)} %bitcast.91, bf16[2048,1,256]{2,0,1:T(8,128)(2,1)S(1)} %bitcast.90, bf16[1280,1,256]{2,0,1:T(8,128)(2,1)S(1)} %bitcast.92, bf16[1280,1,256]{2,0,1:T(8,128)(2,1)S(1)} %bitcast.93), kind=kOutput, calls=%fused_computation | convolution fusion | flops 2688679936 | bytes 8650752 | tf_op jit(solution)/shard_map/dot_general | solution.py:584
  128.5 41.7 %shard_map.181 = bf16[8,40,2048]{2,1,0:T(8,128)(2,1)} custom-call(bf16[8,2,2,40,2048]{4,3,2,1,0:T(8,128)(2,1)} %bitcast.65), custom_call_target="tpu_custom_call" | custom-call | tf_op jit(solution)/shard_map/pallas_call | solution.py:522
  170.2 0.0 copy-start.8
  170.3 2.0 fusion.13
  172.2 0.4 fusion.19.refs_1_
  172.6 0.9 copy.23
  173.5 0.1 copy-done.2
  173.6 45.2 %shard_map.182 = (bf16[8,4,128,256]{3,2,1,0:T(8,128)(2,1)}, bf16[4,128,2048]{2,1,0:T(8,128)(2,1)}, bf16[8,512,256]{2,1,0:T(8,128)(2,1)}, bf16[8,2048]{1,0:T(8,128)(2,1)}) custom-call(bf16[8,128,256]{2,1,0:T(8,128)(2,1)} %bitcast.70, bf16[128,2048]{1,0:T(8,128)(2,1)} %copy-done.2, bf16[512,256]{1,0:T(8,128)(2,1)} %get-tuple-element.29.refs_2_), custom_call_target="tpu_custom_call" | custom-call | tf_op jit(solution)/shard_map/pallas_call | solution.py:366
  218.8 0.0 copy-start.3
  218.8 0.0 copy-start.10
  218.8 0.0 copy-start.7
  218.8 3.8 %fusion.65 = f32[256,256]{1,0:T(8,128)} fusion(bf16[4096,256]{1,0:T(8,128)(2,1)} %bitcast.88, bf16[4096,256]{1,0:T(8,128)(2,1)} %bitcast.89), kind=kOutput, calls=%fused_computation.105 | convolution fusion | flops 536870912 | bytes 4456448 | tf_op jit(solution)/shard_map/dot_general | solution.py:685
  222.6 0.0 copy-done.3
  222.6 0.4 fusion.66
  223.0 1.5 convert_multiply_fusion.4
  224.5 0.7 multiply_select_fusion.1
  225.2 0.9 multiply_convert_fusion.4
  226.1 0.8 multiply_convert_fusion.5
  (26 shorter events, 0.1 us)
Async XLA Ops:
  0.6 112.2 %copy-start = (bf16[1,256,2048]{2,1,0:T(8,128)(2,1)S(1)}, bf16[1,256,2048]{2,1,0:T(8,128)(2,1)}, u32[]{:S(2)}) copy-start(bf16[1,256,2048]{2,1,0:T(8,128)(2,1)} %param.20) | copy-start | bytes 3145732
  5.7 1.6 copy-start.1
  5.8 1.6 copy-start.9
  9.0 96.2 %copy-start.4 = (bf16[512,256]{1,0:T(8,128)(2,1)S(1)}, bf16[512,256]{1,0:T(8,128)(2,1)}, u32[]{:S(2)}) copy-start(bf16[512,256]{1,0:T(8,128)(2,1)} %refs_2_.1) | copy-start | bytes 786436
  9.0 96.2 %copy-start.5 = (bf16[512,256]{1,0:T(8,128)(2,1)S(1)}, bf16[512,256]{1,0:T(8,128)(2,1)}, u32[]{:S(2)}) copy-start(bf16[512,256]{1,0:T(8,128)(2,1)} %refs_3_.1) | copy-start | bytes 786436
  9.0 96.4 %copy-start.6 = (bf16[512,256]{1,0:T(8,128)(2,1)S(1)}, bf16[512,256]{1,0:T(8,128)(2,1)}, u32[]{:S(2)}) copy-start(bf16[512,256]{1,0:T(8,128)(2,1)} %refs_4_.1) | copy-start | bytes 786436
  103.8 2.6 %copy-start.11 = (bf16[1,2048,256]{2,1,0:T(8,128)(2,1)S(1)}, bf16[1,2048,256]{2,1,0:T(8,128)(2,1)}, u32[]{:S(2)}) copy-start(bf16[1,2048,256]{2,1,0:T(8,128)(2,1)} %param.18) | copy-start | bytes 3145732
  105.4 5.5 %slice-start = ((s8[5242880]{0:T(1024)(128)(4,1)}), s8[4194304]{0:T(1024)(128)(4,1)S(1)}, s32[]{:S(2)}) async-start(s8[5242880]{0:T(1024)(128)(4,1)} %bitcast.79), calls=%async_computation | async-start | bytes 8388608
  105.4 7.4 %slice-start.2 = ((s8[5242880]{0:T(1024)(128)(4,1)}), s8[4194304]{0:T(1024)(128)(4,1)S(1)}, s32[]{:S(2)}) async-start(s8[5242880]{0:T(1024)(128)(4,1)} %bitcast.84), calls=%async_computation.2 | async-start | bytes 8388608
  106.3 4.9 %slice-start.1 = ((s8[5242880]{0:T(1024)(128)(4,1)}), s8[1048576]{0:T(1024)(128)(4,1)S(1)}, s32[]{:S(2)}) async-start(s8[5242880]{0:T(1024)(128)(4,1)} %bitcast.79), calls=%async_computation.1 | async-start | bytes 2097152
  106.3 4.9 %copy-start.12 = (bf16[1,2048,256]{2,1,0:T(8,128)(2,1)S(1)}, bf16[1,2048,256]{2,1,0:T(8,128)(2,1)}, u32[]{:S(2)}) copy-start(bf16[1,2048,256]{2,1,0:T(8,128)(2,1)} %param.19) | copy-start | bytes 3145732
  106.4 6.5 %slice-start.3 = ((s8[5242880]{0:T(1024)(128)(4,1)}), s8[1048576]{0:T(1024)(128)(4,1)S(1)}, s32[]{:S(2)}) async-start(s8[5242880]{0:T(1024)(128)(4,1)} %bitcast.84), calls=%async_computation.3 | async-start | bytes 2097152
  170.2 2.0 copy-start.8
  172.6 1.0 copy-start.2
  218.8 3.9 %copy-start.3 = (bf16[256,2048]{1,0:T(8,128)(2,1)S(1)}, bf16[256,2048]{1,0:T(8,128)(2,1)}, u32[]{:S(2)}) copy-start(bf16[256,2048]{1,0:T(8,128)(2,1)} %param.21) | copy-start | bytes 3145732
  218.8 3.8 %copy-start.10 = (bf16[8,2048]{1,0:T(8,128)(2,1)S(1)}, bf16[8,2048]{1,0:T(8,128)(2,1)}, u32[]{:S(2)}) copy-start(bf16[8,2048]{1,0:T(8,128)(2,1)} %get-tuple-element.23) | copy-start | bytes 98308
  218.8 4.2 %copy-start.7 = (bf16[4,128,2048]{2,1,0:T(8,128)(2,1)S(1)}, bf16[4,128,2048]{2,1,0:T(8,128)(2,1)}, u32[]{:S(2)}) copy-start(bf16[4,128,2048]{2,1,0:T(8,128)(2,1)} %get-tuple-element.22) | copy-start | bytes 6291460

commit v4 on v3

--- a/solution.py
+++ b/solution.py
@@ -101,7 +101,7 @@
     mate = mate_of(tp_at)
 
     def origin(step):
-        return partner(sp_at, step, sp_count)
+        return lax.rem(sp_at + sp_count - step, sp_count)
 
     def slot_of(which, step, tp_from):
         if which < exchanged:
@@ -112,7 +112,7 @@
         return sources[which].at[sp_at] if which < exchanged else sources[which]
 
     def row_copy(which, step):
-        to = origin(step)
+        to = lax.rem(sp_at + step, sp_count)
         return remote(
             sources[which].at[to],
             results[which].at[sp_at, tp_at],
@@ -285,25 +285,21 @@
         pass_last(which, 0)
     for which in range(exchanged):
 
-        def step_at(place):
-            return lax.rem(place + sp_count - 3, sp_count - 1) + 1
-
         def relay(step, before):
             row_arrival(which, step).wait_recv()
             pass_on(which, step, slot_of(which, step, tp_at))
             pass_last(which, before)
 
         def relay_at(place):
-            relay(step_at(place), step_at(place - 1))
+            relay(place, place - 1)
             if lined and which == 0:
 
                 @pl.when(lax.rem(place, 2) == 0)
                 def _():
                     line_step(place // 2)
 
-        relay(sp_count - 1, 0)
-        loop(2, sp_count, relay_at)
-        pass_last(which, sp_count - 2)
+        loop(1, sp_count, relay_at)
+        pass_last(which, sp_count - 1)
 
     for copy in locals_:
         copy.wait()

time: 227 us -> 222 us (0.978)
  Pallas kernels: 182 us -> 176 us
    pallas_call x2, Pallas kernels: 140 us -> 122 us  [spread(): pl.pallas_call(functools.partial(spread_kernel, sp_count, tp_count, len(e...]
    pallas_call x1, Pallas kernels: 41.7 us -> 54.4 us  [bring_back(): pl.pallas_call(functools.partial(bring_kernel, sp_count, tp_count), out_s...]
where the time goes in v4:
time: 222 us; the launch traced here: 221 us
  Pallas kernels  176 us (79%)
  matrix products  32.8 us (15%)
  other arithmetic  6.51 us (3%)
  local copies, waits for them, and re-layouts  5.03 us (2%)
    pallas_call x2, Pallas kernels, spread(): pl.pallas_call(functools.partial(spread_kernel, sp_count, tp_count, len(e...  122 us
    pallas_call x1, Pallas kernels, bring_back(): pl.pallas_call(functools.partial(bring_kernel, sp_count, tp_count), out_s...  54.4 us
    dot_general x1, matrix products, expert_work(): lax.dot_general(grads_pair, weights_pair, (((1, 2), (1, 2)), ((), ())), p...  4.69 us
    dot_general x1, matrix products, expert_work(): gate_pre = jnp.dot(rows_in, gate_w, preferred_element_type=jnp.float32)  4.59 us

profile of v4, /device:TPU:0, one launch (start us, length us, event | category | flops | bytes accessed | tf_op | source)
XLA Modules:
  0.0 221.3 jit_solution(10209683041229533626)
XLA Ops:
  0.6 0.0 copy-start
  0.7 1.3 fusion.16
  2.0 0.7 constant_dynamic-slice_fusion.1
  2.7 0.1 select_reduce_fusion.1
  2.8 0.7 constant_dynamic-slice_fusion
  3.6 0.8 fusion.64
  4.4 0.1 fusion.44
  4.5 1.3 fusion.17
  5.7 0.0 copy-start.1
  5.8 0.0 copy-start.9
  5.8 1.6 convolution_convert_fusion.1
  7.4 1.7 convolution_convert_fusion
  9.0 78.1 %shard_map.180 = (bf16[8,4,40,2048]{3,2,1,0:T(8,128)(2,1)}, bf16[8,4,40,2048]{3,2,1,0:T(8,128)(2,1)}, bf16[8,256]{1,0:T(8,128)(2,1)}, bf16[8,256]{1,0:T(8,128)(2,1)}, bf16[8,256]{1,0:T(8,128)(2,1)}) custom-call(bf16[8,40,2048]{2,1,0:T(8,128)(2,1)} %bitcast.66, bf16[8,40,2048]{2,1,0:T(8,128)(2,1)} %bitcast.71, bf16[512,256]{1,0:T(8,128)(2,1)} %refs_2_.1, ...), custom_call_target="tpu_custom_call" | custom-call | tf_op jit(solution)/shard_map/pallas_call | solution.py:362
  87.1 0.0 copy-start.11
  87.2 0.8 slice.53
  87.9 0.7 slice.54
  88.6 0.0 copy-done.4
  88.6 0.2 multiply_select_fusion
  88.8 0.0 slice-start
  88.8 0.0 slice-start.2
  88.8 0.9 fusion.33
  89.7 4.6 %fusion.23 = f32[1280,256]{1,0:T(8,128)S(1)} fusion(bf16[1280,2048]{1,0:T(8,128)(2,1)} %bitcast.78, bf16[1,2048,256]{2,1,0:T(8,128)(2,1)S(1)} %copy-done.11), kind=kOutput, calls=%fused_computation.41 | convolution fusion | flops 1342177280 | bytes 7602176 | tf_op jit(solution)/shard_map/dot_general | solution.py:557
  94.3 0.0 slice-done
  94.3 0.3 slice-done.1
  94.6 1.5 fusion.25
  96.2 0.0 copy-done
  96.2 0.0 slice-done.2
  96.2 0.0 slice-done.3
  96.2 2.1 multiply_convert_fusion.1
  98.3 2.9 %convolution_bitcast_fusion = f32[1,256,2048]{2,1,0:T(8,128)} fusion(bf16[1280,2048]{1,0:T(8,128)(2,1)S(1)} %bitcast.87, f32[1280,256]{1,0:T(8,128)S(1)} %fusion.25, f32[1280,256]{1,0:T(8,128)S(1)} %fusion.23), kind=kOutput, calls=%fused_computation.1 | convolution fusion | flops 1344143360 | bytes 9961472 | tf_op jit(solution)/shard_map/dot_general | solution.py:562
  101.2 3.0 %convolution_bitcast_fusion.1 = f32[1,2048,256]{2,1,0:T(8,128)} fusion(bf16[1280,2048]{1,0:T(8,128)(2,1)S(1)} %bitcast.82, bf16[1280,256]{1,0:T(8,128)(2,1)S(1)} %get-tuple-element.31), kind=kOutput, calls=%fused_computation.2 | convolution fusion | flops 1342177280 | bytes 7995392 | tf_op jit(solution)/shard_map/dot_general | solution.py:575
  104.2 3.0 %convolution_bitcast_fusion.2 = f32[1,2048,256]{2,1,0:T(8,128)} fusion(bf16[1280,2048]{1,0:T(8,128)(2,1)S(1)} %bitcast.83, bf16[1280,256]{1,0:T(8,128)(2,1)S(1)} %get-tuple-element.32), kind=kOutput, calls=%fused_computation.3 | convolution fusion | flops 1342177280 | bytes 7995392 | tf_op jit(solution)/shard_map/dot_general | solution.py:572
  107.2 4.7 %bitcast_convert_fusion = bf16[1280,2048]{1,0:T(8,128)(2,1)} fusion(bf16[2048,1,256]{2,0,1:T(8,128)(2,1)S(1)} %bitcast.91, bf16[2048,1,256]{2,0,1:T(8,128)(2,1)S(1)} %bitcast.90, bf16[1280,1,256]{2,0,1:T(8,128)(2,1)S(1)} %bitcast.92, bf16[1280,1,256]{2,0,1:T(8,128)(2,1)S(1)} %bitcast.93), kind=kOutput, calls=%fused_computation | convolution fusion | flops 2688679936 | bytes 8650752 | tf_op jit(solution)/shard_map/dot_general | solution.py:580
  111.9 54.4 %shard_map.181 = bf16[8,40,2048]{2,1,0:T(8,128)(2,1)} custom-call(bf16[8,2,2,40,2048]{4,3,2,1,0:T(8,128)(2,1)} %bitcast.65), custom_call_target="tpu_custom_call" | custom-call | tf_op jit(solution)/shard_map/pallas_call | solution.py:518
  166.3 0.0 copy-start.8
  166.3 2.0 fusion.13
  168.3 0.0 copy-done.8
  168.3 0.4 fusion.19.refs_1_
  168.7 0.9 copy.23
  169.6 0.1 copy-done.2
  169.6 43.6 %shard_map.182 = (bf16[8,4,128,256]{3,2,1,0:T(8,128)(2,1)}, bf16[4,128,2048]{2,1,0:T(8,128)(2,1)}, bf16[8,512,256]{2,1,0:T(8,128)(2,1)}, bf16[8,2048]{1,0:T(8,128)(2,1)}) custom-call(bf16[8,128,256]{2,1,0:T(8,128)(2,1)} %bitcast.70, bf16[128,2048]{1,0:T(8,128)(2,1)} %copy-done.2, bf16[512,256]{1,0:T(8,128)(2,1)} %get-tuple-element.29.refs_2_), custom_call_target="tpu_custom_call" | custom-call | tf_op jit(solution)/shard_map/pallas_call | solution.py:362
  213.2 0.0 copy-start.3
  213.2 3.8 %fusion.65 = f32[256,256]{1,0:T(8,128)} fusion(bf16[4096,256]{1,0:T(8,128)(2,1)} %bitcast.88, bf16[4096,256]{1,0:T(8,128)(2,1)} %bitcast.89), kind=kOutput, calls=%fused_computation.105 | convolution fusion | flops 536870912 | bytes 4456448 | tf_op jit(solution)/shard_map/dot_general | solution.py:681
  217.1 0.4 fusion.66
  217.4 1.5 convert_multiply_fusion.4
  218.9 0.7 multiply_select_fusion.1
  219.6 0.9 multiply_convert_fusion.4
  220.5 0.8 multiply_convert_fusion.5
  (26 shorter events, 0.1 us)
Async XLA Ops:
  0.6 95.6 %copy-start = (bf16[1,256,2048]{2,1,0:T(8,128)(2,1)S(1)}, bf16[1,256,2048]{2,1,0:T(8,128)(2,1)}, u32[]{:S(2)}) copy-start(bf16[1,256,2048]{2,1,0:T(8,128)(2,1)} %param.20) | copy-start | bytes 3145732
  5.7 1.6 copy-start.1
  5.8 1.6 copy-start.9
  9.0 79.6 %copy-start.4 = (bf16[512,256]{1,0:T(8,128)(2,1)S(1)}, bf16[512,256]{1,0:T(8,128)(2,1)}, u32[]{:S(2)}) copy-start(bf16[512,256]{1,0:T(8,128)(2,1)} %refs_2_.1) | copy-start | bytes 786436
  9.0 79.6 %copy-start.5 = (bf16[512,256]{1,0:T(8,128)(2,1)S(1)}, bf16[512,256]{1,0:T(8,128)(2,1)}, u32[]{:S(2)}) copy-start(bf16[512,256]{1,0:T(8,128)(2,1)} %refs_3_.1) | copy-start | bytes 786436
  9.0 79.7 %copy-start.6 = (bf16[512,256]{1,0:T(8,128)(2,1)S(1)}, bf16[512,256]{1,0:T(8,128)(2,1)}, u32[]{:S(2)}) copy-start(bf16[512,256]{1,0:T(8,128)(2,1)} %refs_4_.1) | copy-start | bytes 786436
  87.1 2.6 %copy-start.11 = (bf16[1,2048,256]{2,1,0:T(8,128)(2,1)S(1)}, bf16[1,2048,256]{2,1,0:T(8,128)(2,1)}, u32[]{:S(2)}) copy-start(bf16[1,2048,256]{2,1,0:T(8,128)(2,1)} %param.18) | copy-start | bytes 3145732
  88.8 5.5 %slice-start = ((s8[5242880]{0:T(1024)(128)(4,1)}), s8[4194304]{0:T(1024)(128)(4,1)S(1)}, s32[]{:S(2)}) async-start(s8[5242880]{0:T(1024)(128)(4,1)} %bitcast.79), calls=%async_computation | async-start | bytes 8388608
  88.8 7.4 %slice-start.2 = ((s8[5242880]{0:T(1024)(128)(4,1)}), s8[4194304]{0:T(1024)(128)(4,1)S(1)}, s32[]{:S(2)}) async-start(s8[5242880]{0:T(1024)(128)(4,1)} %bitcast.84), calls=%async_computation.2 | async-start | bytes 8388608
  89.7 4.9 %slice-start.1 = ((s8[5242880]{0:T(1024)(128)(4,1)}), s8[1048576]{0:T(1024)(128)(4,1)S(1)}, s32[]{:S(2)}) async-start(s8[5242880]{0:T(1024)(128)(4,1)} %bitcast.79), calls=%async_computation.1 | async-start | bytes 2097152
  89.7 4.9 %copy-start.12 = (bf16[1,2048,256]{2,1,0:T(8,128)(2,1)S(1)}, bf16[1,2048,256]{2,1,0:T(8,128)(2,1)}, u32[]{:S(2)}) copy-start(bf16[1,2048,256]{2,1,0:T(8,128)(2,1)} %param.19) | copy-start | bytes 3145732
  89.7 6.5 %slice-start.3 = ((s8[5242880]{0:T(1024)(128)(4,1)}), s8[1048576]{0:T(1024)(128)(4,1)S(1)}, s32[]{:S(2)}) async-start(s8[5242880]{0:T(1024)(128)(4,1)} %bitcast.84), calls=%async_computation.3 | async-start | bytes 2097152
  166.3 2.0 copy-start.8
  168.7 1.0 copy-start.2
  213.2 3.9 %copy-start.3 = (bf16[256,2048]{1,0:T(8,128)(2,1)S(1)}, bf16[256,2048]{1,0:T(8,128)(2,1)}, u32[]{:S(2)}) copy-start(bf16[256,2048]{1,0:T(8,128)(2,1)} %param.21) | copy-start | bytes 3145732
  213.2 3.8 %copy-start.10 = (bf16[8,2048]{1,0:T(8,128)(2,1)S(1)}, bf16[8,2048]{1,0:T(8,128)(2,1)}, u32[]{:S(2)}) copy-start(bf16[8,2048]{1,0:T(8,128)(2,1)} %get-tuple-element.23) | copy-start | bytes 98308
  213.2 4.2 %copy-start.7 = (bf16[4,128,2048]{2,1,0:T(8,128)(2,1)S(1)}, bf16[4,128,2048]{2,1,0:T(8,128)(2,1)}, u32[]{:S(2)}) copy-start(bf16[4,128,2048]{2,1,0:T(8,128)(2,1)} %get-tuple-element.22) | copy-start | bytes 6291460
